TPU v7x, 256 devices: a whole 4x4x8 slice. The times are simulated.
256 devices in a mesh: fs: 32 (over z, y), tp: 8 (over x, core).
Axes of the slice: x: 4, y: 4, z: 8, core: 2. Of those that a mesh axis runs over, the one named last changes fastest.
Arguments:
- tokens: bfloat16 [8192, 2048], P('fs'), may hold values from -6 to 6
- routes: int32 [8192, 6], P('fs'), may hold values from 0 to 31, all different within a row; in each aligned block of 256 rows (0 to 255, 256 to 511, ...) at most 80 rows name the same one
- route_weights: float32 [8192, 6], P('fs'), may hold values from 0.1 to 1
- norm_gain: float32 [2048], P('fs'), may hold values from 0.1 to 1.9
- expert_gate: float32 [32, 2048, 1024], P(None, 'fs', 'tp'), may hold values from -0.125 to 0.125
- expert_up: float32 [32, 2048, 1024], P(None, 'fs', 'tp'), may hold values from -0.125 to 0.125
- expert_down: float32 [32, 2048, 1024], P(None, 'fs', 'tp'), may hold values from -0.1875 to 0.1875
- shared_gate: float32 [2048, 1024], P('fs', 'tp'), may hold values from -0.125 to 0.125
- shared_up: float32 [2048, 1024], P('fs', 'tp'), may hold values from -0.125 to 0.125
- shared_down: float32 [2048, 1024], P('fs', 'tp'), may hold values from -0.1875 to 0.1875
Outputs:
- layer_output: bfloat16 [8192, 2048], P('fs', 'tp')
- sample_gate: bfloat16 [32, 2048, 1024], P('fs', None, 'tp')
- sample_up: bfloat16 [32, 2048, 1024], P('fs', None, 'tp')
- sample_down: bfloat16 [32, 2048, 1024], P('fs', None, 'tp')
- common_gate: bfloat16 [2048, 1024], P(None, 'tp')
- common_up: bfloat16 [2048, 1024], P(None, 'tp')
- common_down: bfloat16 [2048, 1024], P(None, 'tp')
Inputs may be any that keep to these rules, and one draw needn't show every extreme that they name: `routes`: each row names 6 different experts. In each aligned block of 256 rows (the rows of one index of fs) no expert is named by more than 80 rows, a bound that some expert reaches in some blocks.
All inputs are finite; a program needn't handle non-finite values.
Results may differ from a plain program's by a relative error of at most 0.015.
Values may be sent and summed in bfloat16 or wider, within the bound.
A program may use at most 128 MiB of HBM per device.

v0:
```python
import jax
import jax.numpy as jnp
from jax import lax
from jax.sharding import PartitionSpec as P

EPSILON = 1e-06


def in_one_piece(arrays, axis, split_dim, concat_dim, along):
    both = jnp.concatenate(arrays, axis=along)
    out, at, done = (
        lax.all_to_all(both, axis, split_axis=split_dim, concat_axis=concat_dim, tiled=True),
        0,
        [],
    )
    for a in arrays:
        done.append(lax.slice_in_dim(out, at, at + a.shape[along], axis=along))
        at += a.shape[along]
    return tuple(done)


def side_by_side(arrays, axis, dim, along):
    widths = [a.shape[along] for a in arrays]
    both = jnp.concatenate(arrays, axis=along)
    out = lax.all_gather(both, axis, axis=dim, tiled=True)
    return tuple(jnp.split(out, [sum(widths[:k]) for k in range(1, len(widths))], axis=along))


def in_blocks(array, dim, peers):
    before, after = (array.shape[:dim], array.shape[dim + 1 :])
    return jnp.moveaxis(array.reshape(*before, peers, -1, *after), dim, 0)


def summed_on_arrival(array, axis, dim):
    peers = lax.axis_size(axis)
    tiles = lax.all_to_all(in_blocks(array, dim, peers), axis, 0, 0, tiled=True)
    return jnp.sum(tiles.astype(jnp.float32), axis=0)


def normalize(tokens):
    values = tokens.astype(jnp.float32)
    scale = lax.rsqrt(jnp.mean(values * values, axis=-1, keepdims=True) + EPSILON)
    return (values * scale).astype(jnp.bfloat16)


def slot_table(routes, experts, capacity):
    flat_route = routes.reshape(-1)
    member = (flat_route[:, None] == jnp.arange(experts, dtype=jnp.int32)[None, :]).astype(
        jnp.int32
    )
    before = jnp.sum((jnp.cumsum(member, axis=0) - member) * member, axis=1)
    return flat_route * capacity + before


def body(
    tokens,
    routes,
    route_weights,
    norm_gain,
    expert_gate,
    expert_up,
    expert_down,
    shared_gate,
    shared_up,
    shared_down,
):
    gain_rows = norm_gain[None, :, None]
    rounded = (
        (expert_gate * gain_rows).astype(jnp.bfloat16),
        (expert_up * gain_rows).astype(jnp.bfloat16),
        expert_down.astype(jnp.bfloat16),
    )
    sample_gate, sample_up, sample_down = in_one_piece(
        (rounded[0], rounded[1], rounded[2]), "fs", 0, 1, 2
    )
    gate_rows = sample_gate[0]
    up_rows = sample_up[0]
    down_rows = sample_down[0]
    normed = normalize(tokens)
    tok_rows, width = normed.shape
    picks = routes.shape[1]
    experts = expert_gate.shape[0]
    tp_count = lax.axis_size("tp")
    capacity = min(tok_rows, tp_count * max(1, tok_rows * picks * 5 // (3 * experts * tp_count)))
    slots = slot_table(routes, experts, capacity)
    sources = (
        jnp.full((experts * capacity,), tok_rows, jnp.int32)
        .at[slots]
        .set(jnp.arange(tok_rows * picks, dtype=jnp.int32) // picks)
    )
    padded = jnp.concatenate([normed, jnp.zeros((1, width), jnp.bfloat16)], axis=0)
    outgoing = padded[sources].reshape(experts, capacity, width)
    shared_rounded = (
        (shared_gate * norm_gain[:, None]).astype(jnp.bfloat16),
        (shared_up * norm_gain[:, None]).astype(jnp.bfloat16),
        shared_down.astype(jnp.bfloat16),
    )
    common_gate, common_up, common_down = side_by_side(
        (shared_rounded[0], shared_rounded[1], shared_rounded[2]), "fs", 0, 1
    )
    shared_gate_act = jnp.dot(normed, common_gate, preferred_element_type=jnp.float32)
    shared_up_act = jnp.dot(normed, common_up, preferred_element_type=jnp.float32)
    shared_hidden = (jax.nn.silu(shared_gate_act) * shared_up_act).astype(jnp.bfloat16)
    shared_terms = jnp.einsum(
        "th,dh->td", shared_hidden, common_down, preferred_element_type=jnp.float32
    )
    share = capacity // tp_count
    whole_gate, whole_up, whole_down = side_by_side((gate_rows, up_rows, down_rows), "tp", 1, 0)
    own_share = lax.dynamic_slice_in_dim(outgoing, lax.axis_index("tp") * share, share, 1)
    block = lax.all_to_all(own_share, "fs", split_axis=0, concat_axis=0, tiled=True)
    flat = block.reshape(-1, width)
    gate = jnp.dot(flat, whole_gate, preferred_element_type=jnp.float32)
    upward = jnp.dot(flat, whole_up, preferred_element_type=jnp.float32)
    hidden = (jax.nn.silu(gate) * upward).astype(jnp.bfloat16)
    parts = jnp.einsum(
        "rbf,dbf->rbd",
        hidden.reshape(flat.shape[0], tp_count, -1),
        whole_down.reshape(width, tp_count, -1),
        preferred_element_type=jnp.float32,
    ).astype(jnp.bfloat16)
    parts = lax.optimization_barrier(parts)
    total = jnp.sum(parts.astype(jnp.float32), axis=1).astype(jnp.bfloat16)
    results = total.reshape(block.shape[0], block.shape[1], width)
    back = lax.all_to_all(results, "fs", split_axis=0, concat_axis=0, tiled=True).reshape(
        experts * share, width
    )
    position = slots % capacity
    owner = position // share
    local = slots // capacity * share + position % share
    taken = back[local].astype(jnp.float32).reshape(tok_rows, picks, width)
    keep = (owner == lax.axis_index("tp")).astype(jnp.float32).reshape(tok_rows, picks)
    routed_part = jnp.sum(taken * (route_weights * keep)[:, :, None], axis=1)
    shared_part = lax.optimization_barrier(shared_terms.astype(jnp.bfloat16)).astype(jnp.float32)
    layer_output = summed_on_arrival(
        (routed_part + shared_part).astype(jnp.bfloat16), "tp", 1
    ).astype(jnp.bfloat16)
    return (layer_output, sample_gate, sample_up, sample_down, common_gate, common_up, common_down)


def solution(mesh):
    return jax.shard_map(
        body,
        mesh=mesh,
        in_specs=(
            P("fs", None),
            P("fs", None),
            P("fs", None),
            P("fs"),
            P(None, "fs", "tp"),
            P(None, "fs", "tp"),
            P(None, "fs", "tp"),
            P("fs", "tp"),
            P("fs", "tp"),
            P("fs", "tp"),
        ),
        out_specs=(
            P("fs", "tp"),
            P("fs", None, "tp"),
            P("fs", None, "tp"),
            P("fs", None, "tp"),
            P(None, "tp"),
            P(None, "tp"),
            P(None, "tp"),
        ),
        check_vma=False,
    )
```

profile of v0, /device:TPU:1, one launch (start us, length us, event | category | flops | bytes accessed | tf_op | source)
XLA Modules:
  0.0 305.8 jit_solution(906326858509887982)
XLA Ops:
  7.2 1.4 convert_element_type.67
  8.7 1.6 multiply_convert_fusion.1
  10.3 0.2 pad_maximum_fusion
  10.5 50.4 %all_to_all.27 = bf16[32,64,384]{2,1,0:T(8,128)(2,1)S(1)} all-to-all(bf16[32,64,384]{2,1,0:T(8,128)(2,1)S(1)} %pad_maximum_fusion), channel_id=1, replica_groups=mesh['fs'=32,'tp'=8] {'fs'}, dimensions={0} | all-to-all | bytes 3145728 | tf_op jit(solution)/shard_map/all_to_all | solution.py:12
  60.9 0.3 fusion.42
  61.3 0.8 copy-done.5
  62.0 0.2 copy-done.6
  62.2 0.2 copy-done.7
  62.4 1.3 pad_maximum_fusion.1
  63.7 0.1 copy.61
  63.9 0.1 eq.39
  64.2 9.1 %reduce-window.6 = s32[32,12,128]{2,1,0:T(8,128)S(1)} reduce-window(s32[32,12,128]{2,1,0:T(8,128)S(1)} %fusion.18, s32[]{:T(128)} %constant.66.clone.1), window={size=1x1x128 pad=0_0x0_0x127_0}, to_apply=%region_1.0 | reduce-window | flops 6242304 | bytes 393220 | tf_op jit(solution)/shard_map/reduce-window
  73.4 0.2 copy.63
  73.7 0.1 copy.60
  73.9 0.1 mul.116
  74.0 0.3 fusion.4
  74.3 0.2 fusion.5
  75.1 6.2 %scatter_custom_fusion = s32[2560]{0:T(1024)S(1)} fusion(s32[1536]{0:T(1024)S(1)} %get-tuple-element.15, s32[1536]{0:T(1024)S(1)} %add_select_fusion.2, s32[]{:T(128)} %constant.64.clone.1), kind=kCustom, calls=%fused_computation.72 | custom fusion | bytes 10244 | tf_op jit(solution)/shard_map/scatter | solution.py:89
  81.3 10.8 %gather_fusion = bf16[2560,2048]{1,0:T(8,128)(2,1)} fusion(bf16[257,2048]{1,0:T(8,128)(2,1)S(1)} %concatenate.14, s32[3072]{0:T(1024)S(1)} %pad_clamp_fusion), kind=kCustom, calls=%fused_computation | custom fusion | bytes 20981760 | tf_op jit(solution)/shard_map/gather | solution.py:92
  92.1 4.2 %constant_dynamic-slice_fusion = bf16[32,10,2048]{2,1,0:T(8,128)(2,1)} fusion(bf16[32,80,2048]{2,1,0:T(8,128)(2,1)} %bitcast.48, s32[]{:T(128)S(6)} %select_n.76), kind=kLoop, calls=%fused_computation.76 | loop fusion | bytes 2621444 | tf_op jit(solution)/shard_map/dynamic_slice | solution.py:109
  96.3 5.7 %all-to-all-start.1 = ((bf16[32,10,2048]{2,1,0:T(8,128)(2,1)}), bf16[32,10,2048]{2,1,0:T(8,128)(2,1)}, u32[]{:S(2)}, u32[]{:S(2)}) async-start(bf16[32,10,2048]{2,1,0:T(8,128)(2,1)} %constant_dynamic-slice_fusion), calls=%async_computation.1 | async-start | bytes 4194304 | tf_op jit(solution)/shard_map/all_to_all | solution.py:110
  102.1 0.2 all-gather.5.cloned.1.call-start
  102.4 0.6 pad_maximum_fusion.2
  103.1 46.6 %all-to-all-done.1 = bf16[32,10,2048]{2,1,0:T(8,128)(2,1)} async-done(((bf16[32,10,2048]{2,1,0:T(8,128)(2,1)}), bf16[32,10,2048]{2,1,0:T(8,128)(2,1)}, u32[]{:S(2)}, u32[]{:S(2)}) %all-to-all-start.1) | async-done | bytes 1310752 | tf_op jit(solution)/shard_map/all_to_all | solution.py:110
  149.7 2.5 reshape.181
  152.2 4.6 %split.26 = bf16[2048,1024]{1,0:T(8,128)(2,1)} slice(bf16[6144,1024]{1,0:T(8,128)(2,1)} %all-gather.3.cloned.1.call-done), slice={[4096:6144], [0:1024]} | slice | bytes 8388608 | tf_op jit(solution)/shard_map/split | solution.py:26
  156.8 6.5 %copy.59 = bf16[2048,1024]{0,1:T(8,128)(2,1)} copy(bf16[2048,1024]{1,0:T(8,128)(2,1)} %split.26) | data formatting | bytes 8388608 | tf_op jit(solution)/shard_map/split | solution.py:26
  163.3 3.7 %fusion.2 = f32[320,1024]{1,0:T(8,128)S(1)} fusion(bf16[320,2048]{1,0:T(8,128)(2,1)S(1)} %reshape.181, bf16[6144,1024]{1,0:T(8,128)(2,1)} %all-gather.3.cloned.1.call-done), kind=kOutput, calls=%fused_computation.7 | convolution fusion | flops 1342177280 | bytes 6815744 | tf_op jit(solution)/shard_map/dot_general | solution.py:112
  167.1 4.0 %fusion.12 = bf16[40,8,8,128]{3,2,1,0:T(8,128)(2,1)S(1)} fusion(bf16[320,2048]{1,0:T(8,128)(2,1)S(1)} %reshape.181, bf16[6144,1024]{1,0:T(8,128)(2,1)} %all-gather.3.cloned.1.call-done, f32[320,1024]{1,0:T(8,128)S(1)} %fusion.2), kind=kOutput, calls=%fused_computation.19 | convolution fusion | flops 1344143360 | bytes 7471104 | tf_op jit(solution)/shard_map/dot_general | solution.py:113
  171.1 5.5 %convert_bitcast_fusion = bf16[320,8,2048]{2,0,1:T(8,128)(2,1)} fusion(bf16[2048,8,128]{0,2,1:T(8,128)(2,1)S(1)} %bitcast.47, bf16[40,8,8,128]{3,2,1,0:T(8,128)(2,1)S(1)} %fusion.12), kind=kOutput, calls=%fused_computation.4 | convolution fusion | flops 1347420160 | bytes 15335424 | tf_op jit(solution)/shard_map/rbf,dbf->rbd/dot_general | solution.py:115
  176.6 6.4 %reduce_sum.58 = bf16[320,2048]{1,0:T(8,128)(2,1)S(1)} reduce(bf16[320,8,2048]{2,0,1:T(8,128)(2,1)} %convert_bitcast_fusion, bf16[]{:T(256)} %constant.63.clone.1), dimensions={1}, to_apply=%region_5.6 | reduce | flops 4587520 | bytes 11796482 | tf_op jit(solution)/shard_map/reduce_sum | solution.py:122
  183.0 1.5 reshape.183
  184.6 7.5 %all-to-all-start.2 = ((bf16[32,10,2048]{2,1,0:T(8,128)(2,1)}), bf16[32,10,2048]{2,1,0:T(8,128)(2,1)}, u32[]{:S(2)}, u32[]{:S(2)}) async-start(bf16[32,10,2048]{2,1,0:T(8,128)(2,1)} %reshape.183), calls=%async_computation.2 | async-start | bytes 4194304 | tf_op jit(solution)/shard_map/all_to_all | solution.py:124
  192.1 0.1 reduce_sum.59
  192.4 0.1 copy.68
  192.5 29.4 %all-gather.5.cloned.1.call-done = bf16[2048,384]{1,0:T(8,128)(2,1)} async-done(((bf16[64,384]{1,0:T(8,128)(2,1)}), bf16[2048,384]{1,0:T(8,128)(2,1)}) %all-gather.5.cloned.1.call-update) | async-done | bytes 1572880 | tf_op jit(solution)/shard_map/all_gather | solution.py:25
  221.9 1.5 fusion.41
  223.4 0.4 fusion.43
  223.8 0.3 copy-done.4
  224.1 0.8 convolution_convert_fusion
  224.9 21.1 %all-to-all-done.2 = bf16[32,10,2048]{2,1,0:T(8,128)(2,1)} async-done(((bf16[32,10,2048]{2,1,0:T(8,128)(2,1)}), bf16[32,10,2048]{2,1,0:T(8,128)(2,1)}, u32[]{:S(2)}, u32[]{:S(2)}) %all-to-all-start.2) | async-done | bytes 1310752 | tf_op jit(solution)/shard_map/all_to_all | solution.py:124
  246.0 2.5 reshape.184
  248.5 7.1 %gather_fusion.1 = bf16[1536,2048]{1,0:T(8,128)(2,1)} fusion(bf16[320,2048]{1,0:T(8,128)(2,1)S(1)} %reshape.184, s32[2048]{0:T(1024)S(1)} %pad_clamp_fusion.1), kind=kCustom, calls=%fused_computation.1 | custom fusion | bytes 12589056 | tf_op jit(solution)/shard_map/gather | solution.py:130
  255.6 11.7 %reshape.186 = f32[256,6,2048]{2,1,0:T(8,128)} reshape(bf16[1536,2048]{1,0:T(8,128)(2,1)} %gather_fusion.1) | data formatting | bytes 18874368 | tf_op jit(solution)/shard_map/convert_element_type | solution.py:130
  267.3 9.4 %multiply_reduce_fusion = f32[256,2048]{1,0:T(8,128)S(1)} fusion(f32[256,6,2048]{2,1,0:T(8,128)} %reshape.186, f32[256,6]{1,0:T(8,128)S(1)} %copy.68), kind=kLoop, calls=%fused_computation.3 | loop fusion | flops 5767168 | bytes 14686208 | tf_op jit(solution)/shard_map/reduce_sum | solution.py:132
  276.7 0.3 add_convert_fusion
  277.1 21.1 %all_to_all.28 = bf16[8,256,256]{2,1,0:T(8,128)(2,1)S(1)} all-to-all(bf16[8,256,256]{2,1,0:T(8,128)(2,1)S(1)} %bitcast.50), channel_id=1, replica_groups=mesh['fs'=32,'tp'=8] {'tp'}, dimensions={0} | all-to-all | bytes 2097152 | tf_op jit(solution)/shard_map/all_to_all | solution.py:36
  298.2 0.8 reduce_sum.61
  (50 shorter events, 1.4 us)
Async XLA Ops:
  7.2 1.5 copy-start.8
  7.2 145.0 %all-gather.3.cloned.1.call-start = ((), (), s32[]{:S(2)}) async-start(), calls=%async_computation.4 | async-start | bytes 14155776 | tf_op jit(solution)/shard_map/all_gather | solution.py:25
  61.2 0.8 copy-start.5
  61.2 1.0 copy-start.6
  61.2 1.1 copy-start.7
  62.4 1.4 copy-start.9
  63.7 10.3 %copy-start.1 = (bf16[256,2048]{1,0:T(8,128)(2,1)S(1)}, bf16[256,2048]{1,0:T(8,128)(2,1)}, u32[]{:S(2)}) copy-start(bf16[256,2048]{1,0:T(8,128)(2,1)} %param.10) | copy-start | bytes 3145732
  96.3 6.0 %copy-start.12 = (f32[64,128]{1,0:T(8,128)S(1)}, f32[64,128]{1,0:T(8,128)}, u32[]{:S(2)}) copy-start(f32[64,128]{1,0:T(8,128)} %param.19) | copy-start | bytes 98308
  96.3 6.0 %copy-start.10 = (f32[64,128]{1,0:T(8,128)S(1)}, f32[64,128]{1,0:T(8,128)}, u32[]{:S(2)}) copy-start(f32[64,128]{1,0:T(8,128)} %param.17) | copy-start | bytes 98308
  96.3 6.0 %copy-start.11 = (f32[64,128]{1,0:T(8,128)S(1)}, f32[64,128]{1,0:T(8,128)}, u32[]{:S(2)}) copy-start(f32[64,128]{1,0:T(8,128)} %param.18) | copy-start | bytes 98308
  96.3 6.0 %copy-start.14 = (f32[64]{0:T(128)S(1)}, f32[64]{0:T(128)}, u32[]{:S(2)}) copy-start(f32[64]{0:T(128)} %param.13) | copy-start | bytes 772
  96.3 53.4 %all-to-all-start.1 = ((bf16[32,10,2048]{2,1,0:T(8,128)(2,1)}), bf16[32,10,2048]{2,1,0:T(8,128)(2,1)}, u32[]{:S(2)}, u32[]{:S(2)}) async-start(bf16[32,10,2048]{2,1,0:T(8,128)(2,1)} %constant_dynamic-slice_fusion), calls=%async_computation.1 | async-start | bytes 4194304 | tf_op jit(solution)/shard_map/all_to_all | solution.py:110
  102.1 119.8 %all-gather.5.cloned.1.call-start = ((), (), s32[]{:S(2)}) async-start(), calls=%async_computation.5 | async-start | bytes 1622016 | tf_op jit(solution)/shard_map/all_gather | solution.py:25
  167.0 4.0 %copy-start = (bf16[2048,1024]{0,1:T(8,128)(2,1)S(1)}, bf16[2048,1024]{0,1:T(8,128)(2,1)}, u32[]{:S(2)}) copy-start(bf16[2048,1024]{0,1:T(8,128)(2,1)} %copy.59) | copy-start | bytes 12582916
  184.5 7.8 %copy-start.13 = (f32[256,6]{0,1:T(8,128)S(1)}, f32[256,6]{0,1:T(8,128)}, u32[]{:S(2)}) copy-start(f32[256,6]{0,1:T(8,128)} %param.12) | copy-start | bytes 18436
  184.6 61.5 %all-to-all-start.2 = ((bf16[32,10,2048]{2,1,0:T(8,128)(2,1)}), bf16[32,10,2048]{2,1,0:T(8,128)(2,1)}, u32[]{:S(2)}, u32[]{:S(2)}) async-start(bf16[32,10,2048]{2,1,0:T(8,128)(2,1)} %reshape.183), calls=%async_computation.2 | async-start | bytes 4194304 | tf_op jit(solution)/shard_map/all_to_all | solution.py:124
  223.4 0.8 copy-start.4
  223.4 1.6 copy-start.2
  223.4 1.6 copy-start.3
Sparse Core Ops, SparseCore 0:
  63.8 72.5 all-gather.2
  139.6 82.2 all-gather.4
where the time goes:
time: 308 us; the launch traced here: 306 us
  waiting for transfers between devices  97.1 us (32%)
  blocking collectives  71.5 us (23%)
  local copies, waits for them, and re-layouts  62.6 us (20%)
  other arithmetic  32.2 us (10%)
  between operations  14.5 us (5%)
  matrix products  14.4 us (5%)
  starting transfers between devices  13.6 us (4%)
    all_to_all x1, blocking collectives, in_one_piece(): lax.all_to_all(both, axis, split_axis=split_dim, concat_axis=concat_dim,...  50.4 us
    all_to_all x1, waiting for transfers between devices, body(): lax.all_to_all(own_share, 'fs', split_axis=0, concat_axis=0, tiled=True)  46.6 us
    all_gather x2, waiting for transfers between devices, side_by_side(): out = lax.all_gather(both, axis, axis=dim, tiled=True)  29.4 us
    all_to_all x1, blocking collectives, summed_on_arrival(): tiles = lax.all_to_all(in_blocks(array, dim, peers), axis, 0, 0, tiled=True)  21.1 us
    all_to_all x1, waiting for transfers between devices, body(): lax.all_to_all(results, 'fs', split_axis=0, concat_axis=0, tiled=True)  21.1 us
    split x3, local copies, waits for them, and re-layouts, side_by_side(): jnp.split(out, [sum(widths[:k]) for k in range(1, len(widths))], axis=along)  12.6 us
    convert_element_type x1, local copies, waits for them, and re-layouts, body(): taken = back[local].astype(jnp.float32).reshape(tok_rows, picks, width)  11.7 us
    gather x1, local copies, waits for them, and re-layouts, body(): outgoing = padded[sources].reshape(experts, capacity, width)  10.8 us
  transfers between devices with their start and end apart: 4, of which 3 were waited for; matrix products, arithmetic and copies ran while one was open for 23% of the time, Pallas kernels for 0%

commit v1 on v0

v1 whole, which is shorter than its diff:
```python
import jax
import jax.numpy as jnp
from jax import lax
from jax.sharding import PartitionSpec as P

EPSILON = 1e-06


def normalize(tokens):
    values = tokens.astype(jnp.float32)
    scale = lax.rsqrt(jnp.mean(values * values, axis=-1, keepdims=True) + EPSILON)
    return (values * scale).astype(jnp.bfloat16)


def body(
    tokens,
    routes,
    route_weights,
    norm_gain,
    expert_gate,
    expert_up,
    expert_down,
    shared_gate,
    shared_up,
    shared_down,
):
    bf16, f32 = jnp.bfloat16, jnp.float32
    tp_count = lax.axis_size("tp")
    me_tp = lax.axis_index("tp")
    experts = expert_gate.shape[0]
    gain_rows = norm_gain[None, :, None]
    packed = jnp.concatenate(
        [
            (expert_gate * gain_rows).astype(bf16),
            (expert_up * gain_rows).astype(bf16),
            expert_down.astype(bf16),
        ],
        axis=2,
    )
    mine = lax.all_to_all(packed, "fs", split_axis=0, concat_axis=1, tiled=True)
    width = expert_gate.shape[2]
    sample_gate, sample_up, sample_down = (
        mine[:, :, i * width : (i + 1) * width] for i in range(3)
    )
    normed = normalize(tokens)
    tok_rows, depth = normed.shape
    share = tok_rows // tp_count
    hits = routes[:, :, None] == jnp.arange(experts, dtype=jnp.int32)[None, None, :]
    dense = jnp.sum(jnp.where(hits, route_weights[:, :, None], 0.0), axis=1)
    own_rows = lax.dynamic_slice_in_dim(normed, me_tp * share, share, 0)
    own_dense = lax.dynamic_slice_in_dim(dense, me_tp * share, share, 0)
    rows = lax.all_gather(own_rows, "fs", axis=0, tiled=True)
    scales = lax.all_to_all(own_dense.T, "fs", split_axis=0, concat_axis=0, tiled=True)
    scales = scales.reshape(-1, 1)

    shared_packed = jnp.concatenate(
        [
            (shared_gate * norm_gain[:, None]).astype(bf16),
            (shared_up * norm_gain[:, None]).astype(bf16),
            shared_down.astype(bf16),
        ],
        axis=1,
    )
    common = lax.all_gather(shared_packed, "fs", axis=0, tiled=True)
    common_gate, common_up, common_down = (
        common[:, i * width : (i + 1) * width] for i in range(3)
    )
    sg = jnp.dot(normed, common_gate, preferred_element_type=f32)
    su = jnp.dot(normed, common_up, preferred_element_type=f32)
    sh = (jax.nn.silu(sg) * su).astype(bf16)
    shared_terms = jnp.einsum("th,dh->td", sh, common_down, preferred_element_type=f32).astype(bf16)
    shared_sum = lax.psum_scatter(shared_terms, "tp", scatter_dimension=0, tiled=True)

    whole = lax.all_gather(mine[0], "tp", axis=0, tiled=False)
    total = jnp.zeros((), f32)
    gate = jnp.einsum("rd,bdh->rbh", rows, whole[:, :, :width], preferred_element_type=f32)
    up = jnp.einsum("rd,bdh->rbh", rows, whole[:, :, width : 2 * width], preferred_element_type=f32)
    hidden = (jax.nn.silu(gate) * up).astype(bf16)
    out = jnp.einsum("rbh,bdh->rd", hidden, whole[:, :, 2 * width :], preferred_element_type=f32)
    weighted = (out * scales).astype(bf16)
    routed = lax.psum_scatter(weighted, "fs", scatter_dimension=0, tiled=True)
    final = (routed.astype(f32) + shared_sum.astype(f32)).astype(bf16)
    layer_output = lax.all_to_all(final, "tp", split_axis=1, concat_axis=0, tiled=True)
    return (layer_output, sample_gate, sample_up, sample_down, common_gate, common_up, common_down)


def solution(mesh):
    return jax.shard_map(
        body,
        mesh=mesh,
        in_specs=(
            P("fs", None),
            P("fs", None),
            P("fs", None),
            P("fs"),
            P(None, "fs", "tp"),
            P(None, "fs", "tp"),
            P(None, "fs", "tp"),
            P("fs", "tp"),
            P("fs", "tp"),
            P("fs", "tp"),
        ),
        out_specs=(
            P("fs", "tp"),
            P("fs", None, "tp"),
            P("fs", None, "tp"),
            P("fs", None, "tp"),
            P(None, "tp"),
            P(None, "tp"),
            P(None, "tp"),
        ),
        check_vma=False,
    )
```

time: 308 us -> 529 us (1.72)
  waiting for transfers between devices: 97.1 us -> 396 us
  local copies, waits for them, and re-layouts: 62.6 us -> 5.4 us
  other arithmetic: 32.2 us -> 8.9 us
  matrix products: 14.4 us -> 27.6 us
    reduce_scatter x0 -> x2, waiting for transfers between devices: none -> 233 us  [the longest x1 224 us: body(): routed = lax.psum_scatter(weighted, 'fs', scatter_dimension=0, tiled=True)]
    all_gather x2 -> x3, waiting for transfers between devices: 29.4 us -> 159 us  [the longest x1 79.8 us: body(): rows = lax.all_gather(own_rows, 'fs', axis=0, tiled=True)]
    all_to_all x2 -> x1, waiting for transfers between devices: 67.7 us -> 4 us  [body(): lax.all_to_all(final, 'tp', split_axis=1, concat_axis=0, tiled=True)]
    gather x2 -> x0, local copies, waits for them, and re-layouts: 17.9 us -> none  [the longest x1 10.8 us: body(): outgoing = padded[sources].reshape(experts, capacity, width)]
    reduce_sum x4 -> x1, other arithmetic: 16.7 us -> 0.03 us  [body(): dense = jnp.sum(jnp.where(hits, route_weights[:, :, None], 0.0), axis=1)]
    dot_general x5 -> x4, matrix products: 14.4 us -> 27.6 us  [the longest x1 15.5 us: body(): jnp.einsum('rbh,bdh->rd', hidden, whole[:, :, 2 * width:], preferred_elem...]
    split x3 -> x0, local copies, waits for them, and re-layouts: 12.6 us -> none  [side_by_side(): jnp.split(out, [sum(widths[:k]) for k in range(1, len(widths))], axis=along)]
    convert_element_type x1 -> x0, local copies, waits for them, and re-layouts: 11.7 us -> none  [body(): taken = back[local].astype(jnp.float32).reshape(tok_rows, picks, width)]
  transfers between devices with their start and end apart: 4 -> 6, of which waited for: 3 -> 6; matrix products, arithmetic and copies ran while one was open for 23% -> 7% of each run, Pallas kernels for 0% -> 0%
where the time goes in v1:
time: 529 us; the launch traced here: 528 us
  waiting for transfers between devices  396 us (75%)
  blocking collectives  66.4 us (13%)
  matrix products  27.6 us (5%)
  between operations  14 us (3%)
  starting transfers between devices  10 us (2%)
  other arithmetic  8.9 us (2%)
  local copies, waits for them, and re-layouts  5.4 us (1%)
    reduce_scatter x1, waiting for transfers between devices, body(): routed = lax.psum_scatter(weighted, 'fs', scatter_dimension=0, tiled=True)  224 us
    all_gather x1, waiting for transfers between devices, body(): rows = lax.all_gather(own_rows, 'fs', axis=0, tiled=True)  79.8 us
    all_gather x1, waiting for transfers between devices, body(): whole = lax.all_gather(mine[0], 'tp', axis=0, tiled=False)  72.4 us
    all_to_all x1, blocking collectives, body(): mine = lax.all_to_all(packed, 'fs', split_axis=0, concat_axis=1, tiled=True)  52.6 us
    dot_general x1, matrix products, body(): jnp.einsum('rbh,bdh->rd', hidden, whole[:, :, 2 * width:], preferred_elem...  15.5 us
    all_to_all x1, blocking collectives, body(): lax.all_to_all(own_dense.T, 'fs', split_axis=0, concat_axis=0, tiled=True)  13.8 us
  transfers between devices with their start and end apart: 6, of which 6 were waited for; matrix products, arithmetic and copies ran while one was open for 7% of the time, Pallas kernels for 0%

profile of v1, /device:TPU:1, one launch (start us, length us, event | category | flops | bytes accessed | tf_op | source)
XLA Modules:
  0.0 528.3 jit_solution(2607383099110861899)
XLA Ops:
  7.2 0.0 copy-start.8
  7.2 0.0 copy-start.4
  7.2 0.0 all-gather.8.cloned.1.call-start
  7.2 0.9 convert_element_type.55
  8.1 0.9 multiply_convert_fusion.4
  9.0 0.6 pad_maximum_fusion.1
  9.6 0.0 all-gather.8.cloned.1.call-update
  9.7 0.0 all-gather.4.cloned.1.call-start
  9.7 1.5 fusion.12
  11.2 1.5 fusion.13
  12.7 0.7 constant_dynamic-slice_fusion.1
  13.4 0.0 all-gather.4.cloned.1.call-update
  13.4 0.0 all-gather.6.cloned.1.call-start
  13.5 0.1 convert_element_type.49
  13.6 1.5 multiply_convert_fusion.2
  15.1 0.0 copy-start.6
  15.1 0.0 copy-start.7
  15.1 0.2 pad_maximum_fusion
  15.3 52.6 %all_to_all.40 = bf16[32,64,384]{2,1,0:T(8,128)(2,1)} all-to-all(bf16[32,64,384]{2,1,0:T(8,128)(2,1)S(1)} %pad_maximum_fusion), channel_id=1, replica_groups=mesh['fs'=32,'tp'=8] {'fs'}, dimensions={0} | all-to-all | bytes 3145728 | tf_op jit(solution)/shard_map/all_to_all | solution.py:40
  67.9 0.0 all-gather.6.cloned.1.call-update
  67.9 0.0 reduce-scatter.5.cloned.1.call-start
  68.0 0.1 constant_dynamic-slice_fusion
  68.1 13.8 %all_to_all.41 = f32[32,1,32]{2,1,0:T(1,128)S(1)} all-to-all(f32[32,1,32]{2,1,0:T(1,128)S(1)} %bitcast.35), channel_id=1, replica_groups=mesh['fs'=32,'tp'=8] {'fs'}, dimensions={0} | all-to-all | bytes 8192 | tf_op jit(solution)/shard_map/all_to_all | solution.py:53
  81.9 0.5 broadcast.22
  82.5 0.7 reduce.3
  83.2 0.1 mul.76
  83.2 6.6 %all-gather.8.cloned.1.call-done = bf16[2048,384]{1,0:T(8,128)(2,1)} async-done(((bf16[64,384]{1,0:T(8,128)(2,1)}), bf16[2048,384]{1,0:T(8,128)(2,1)}) %all-gather.8.cloned.1.call-update) | async-done | bytes 1572880 | tf_op jit(solution)/shard_map/all_gather | solution.py:64
  89.8 1.5 fusion.28
  91.3 0.0 copy-start.1
  91.3 0.0 copy-start.2
  91.3 0.0 copy-start.3
  91.3 0.4 fusion.29
  91.7 1.7 convolution_convert_fusion
  93.5 0.0 reduce-scatter.5.cloned.1.call-update
  93.5 0.0 reduce-scatter.3.cloned.1.call-start
  93.6 79.8 %all-gather.4.cloned.1.call-done = bf16[1024,2048]{1,0:T(8,128)(2,1)} async-done(((bf16[32,2048]{1,0:T(8,128)(2,1)}), bf16[1024,2048]{1,0:T(8,128)(2,1)}) %all-gather.4.cloned.1.call-update) | async-done | bytes 4194320 | tf_op jit(solution)/shard_map/all_gather | solution.py:52
  173.4 72.4 %all-gather.6.cloned.1.call-done = bf16[8,2048,384]{2,1,0:T(8,128)(2,1)} async-done(((bf16[1,2048,384]{2,1,0:T(8,128)(2,1)}), bf16[8,2048,384]{2,1,0:T(8,128)(2,1)}) %all-gather.6.cloned.1.call-update) | async-done | bytes 12582928 | tf_op jit(solution)/shard_map/all_gather | solution.py:74
  245.8 9.9 %fusion.2 = f32[1024,8,128]{2,0,1:T(8,128)} fusion(bf16[8,2048,384]{2,1,0:T(8,128)(2,1)} %all-gather.6.cloned.1.call-done, bf16[1024,2048]{1,0:T(8,128)(2,1)} %all-gather.4.cloned.1.call-done), kind=kOutput, calls=%fused_computation.3 | convolution fusion | flops 4294967296 | bytes 12582912 | tf_op jit(solution)/shard_map/rd,bdh->rbh/dot_general | solution.py:77
  255.7 15.5 %fusion = bf16[1024,2048]{1,0:T(8,128)(2,1)} fusion(bf16[8,2048,384]{2,1,0:T(8,128)(2,1)} %all-gather.6.cloned.1.call-done, f32[1024]{0:T(1024)S(1)} %mul.76, f32[1024,8,128]{2,0,1:T(8,128)} %fusion.2, bf16[1024,2048]{1,0:T(8,128)(2,1)} %all-gather.4.cloned.1.call-done), kind=kOutput, calls=%fused_computation.1 | convolution fusion | flops 8600420352 | bytes 20975616 | tf_op jit(solution)/shard_map/rbh,bdh->rd/dot_general | solution.py:79
  271.2 0.0 reduce-scatter.3.cloned.1.call-update
  271.2 9.4 %reduce-scatter.5.cloned.1.call-done = bf16[32,2048]{1,0:T(8,128)(2,1)} async-done(((bf16[256,2048]{1,0:T(8,128)(2,1)}), bf16[32,2048]{1,0:T(8,128)(2,1)}) %reduce-scatter.5.cloned.1.call-update) | async-done | bytes 131088 | tf_op jit(solution)/shard_map/reduce_scatter | solution.py:72
  280.7 223.7 %reduce-scatter.3.cloned.1.call-done = bf16[32,2048]{1,0:T(8,128)(2,1)} async-done(((bf16[1024,2048]{1,0:T(8,128)(2,1)}), bf16[32,2048]{1,0:T(8,128)(2,1)}) %reduce-scatter.3.cloned.1.call-update) | async-done | bytes 131088 | tf_op jit(solution)/shard_map/reduce_scatter | solution.py:81
  504.4 1.0 add_convert_fusion
  505.4 0.7 copy.30
  506.1 9.8 %all-to-all-start.2 = ((bf16[32,8,256]{2,0,1:T(8,128)(2,1)}), bf16[32,8,256]{2,0,1:T(8,128)(2,1)S(1)}, u32[]{:S(2)}, u32[]{:S(2)}) async-start(bf16[32,8,256]{2,0,1:T(8,128)(2,1)} %bitcast.30), calls=%async_computation.4 | async-start | bytes 262144 | tf_op jit(solution)/shard_map/all_to_all | solution.py:83
  515.9 1.2 fusion.27
  517.2 4.0 all-to-all-done.2
  521.2 0.7 copy.32
  (13 shorter events, 0.1 us)
Async XLA Ops:
  7.2 6.4 %copy-start.8 = (f32[64]{0:T(128)S(1)}, f32[64]{0:T(128)}, u32[]{:S(2)}) copy-start(f32[64]{0:T(128)} %param.13) | copy-start | bytes 772
  7.2 6.3 %copy-start.4 = (f32[32,64,128]{2,1,0:T(8,128)S(1)}, f32[32,64,128]{2,1,0:T(8,128)}, u32[]{:S(2)}) copy-start(f32[32,64,128]{2,1,0:T(8,128)} %param.16) | copy-start | bytes 3145732
  7.2 6.4 %copy-start.5 = (f32[32,64,128]{2,1,0:T(8,128)S(1)}, f32[32,64,128]{2,1,0:T(8,128)}, u32[]{:S(2)}) copy-start(f32[32,64,128]{2,1,0:T(8,128)} %param.14) | copy-start | bytes 3145732
  7.2 82.6 %all-gather.8.cloned.1.call-start = ((), (), s32[]{:S(2)}) async-start(), calls=%async_computation.8 | async-start | bytes 1622016 | tf_op jit(solution)/shard_map/all_gather | solution.py:64
  9.7 163.7 %all-gather.4.cloned.1.call-start = ((), (), s32[]{:S(2)}) async-start(), calls=%async_computation.5 | async-start | bytes 4325376 | tf_op jit(solution)/shard_map/all_gather | solution.py:52
  13.4 232.4 %all-gather.6.cloned.1.call-start = ((), (), s32[]{:S(2)}) async-start(), calls=%async_computation.6 | async-start | bytes 14155776 | tf_op jit(solution)/shard_map/all_gather | solution.py:74
  15.1 52.9 %copy-start.6 = (f32[256,6]{0,1:T(8,128)S(1)}, f32[256,6]{0,1:T(8,128)}, u32[]{:S(2)}) copy-start(f32[256,6]{0,1:T(8,128)} %param.12) | copy-start | bytes 18436
  15.1 52.9 %copy-start.7 = (s32[256,6]{0,1:T(8,128)S(1)}, s32[256,6]{0,1:T(8,128)}, u32[]{:S(2)}) copy-start(s32[256,6]{0,1:T(8,128)} %param.11) | copy-start | bytes 18436
  67.9 212.7 %reduce-scatter.5.cloned.1.call-start = ((), (), s32[]{:S(2)}) async-start(), calls=%async_computation.9 | async-start | bytes 1179648 | tf_op jit(solution)/shard_map/reduce_scatter | solution.py:72
  91.3 164.4 %copy-start.1 = (bf16[2048,128]{1,0:T(8,128)(2,1)}, bf16[2048,128]{1,0:T(8,128)(2,1)S(1)}, u32[]{:S(2)}) copy-start(bf16[2048,128]{1,0:T(8,128)(2,1)S(1)} %get-tuple-element.30) | copy-start | bytes 1572868
  91.3 164.4 %copy-start.2 = (bf16[2048,128]{1,0:T(8,128)(2,1)}, bf16[2048,128]{1,0:T(8,128)(2,1)S(1)}, u32[]{:S(2)}) copy-start(bf16[2048,128]{1,0:T(8,128)(2,1)S(1)} %get-tuple-element.29) | copy-start | bytes 1572868
  91.3 164.4 %copy-start.3 = (bf16[2048,128]{1,0:T(8,128)(2,1)}, bf16[2048,128]{1,0:T(8,128)(2,1)S(1)}, u32[]{:S(2)}) copy-start(bf16[2048,128]{1,0:T(8,128)(2,1)S(1)} %get-tuple-element.28) | copy-start | bytes 1572868
  93.5 410.9 %reduce-scatter.3.cloned.1.call-start = ((), (), s32[]{:S(2)}) async-start(), calls=%async_computation.7 | async-start | bytes 4325376 | tf_op jit(solution)/shard_map/reduce_scatter | solution.py:81
  271.2 244.7 %copy-start = (bf16[32,64,384]{2,1,0:T(8,128)(2,1)S(1)}, bf16[32,64,384]{2,1,0:T(8,128)(2,1)}, u32[]{:S(2)}) copy-start(bf16[32,64,384]{2,1,0:T(8,128)(2,1)} %all_to_all.40) | copy-start | bytes 4718596
  506.1 15.1 %all-to-all-start.2 = ((bf16[32,8,256]{2,0,1:T(8,128)(2,1)}), bf16[32,8,256]{2,0,1:T(8,128)(2,1)S(1)}, u32[]{:S(2)}, u32[]{:S(2)}) async-start(bf16[32,8,256]{2,0,1:T(8,128)(2,1)} %bitcast.30), calls=%async_computation.4 | async-start | bytes 262144 | tf_op jit(solution)/shard_map/all_to_all | solution.py:83
Sparse Core Ops, SparseCore 0:
  11.2 78.6 all-gather.7
  93.0 80.3 all-gather.3
  175.2 70.5 all-gather.5
  248.2 32.4 reduce-scatter.4
  284.4 219.9 reduce-scatter.2

commit v2 on v1

v2 whole, which is shorter than its diff:
```python
import functools
import jax
import jax.numpy as jnp
from jax import lax
from jax.experimental import pallas as pl
from jax.experimental.pallas import tpu as pltpu
from jax.sharding import PartitionSpec as P

MESH = pl.DeviceIdType.MESH
bf16, f32 = jnp.bfloat16, jnp.float32
NZ, NY, NX = 8, 4, 4
COLS = 2048 + 128

A2A = 0
TOKZ = 3
TOKY = 11
SHZ = 15
SHY = 23
XAG = 27
RAZ = 54
RAY = 62
RBY = 66
RBZ = 70
SPX = 78
FIN = 79
NSEM = 80


def rc(src, dst, ssem, rsem, dev):
    return pltpu.make_async_remote_copy(
        src_ref=src, dst_ref=dst, send_sem=ssem, recv_sem=rsem, device_id=dev, device_id_type=MESH
    )


def kernel(
    tok_ref, dense_ref, gain_ref, eg_ref, eu_ref, ed_ref, sg_ref, su_ref, sd_ref,
    lo_out, sg_out, su_out, sd_out, cm_out,
    wsend, w, tk, sh, nb, gbuf, hbuf, ob, ra, ya, yb, zb, sa, sp, sr, fin, lo, send, recv, loc,
):
    fs, tp = lax.axis_index("fs"), lax.axis_index("tp")
    z, y = fs // NY, fs % NY
    x, c = tp // 2, tp % 2

    def at_z(d):
        return ((z + d + NZ) % NZ) * NY + y

    def at_y(d):
        return z * NY + (y + d + NY) % NY

    xr, xl = ((x + 1) % NX) * 2 + c, ((x + NX - 1) % NX) * 2 + c
    mate = x * 2 + 1 - c

    barrier = pltpu.get_barrier_semaphore()

    def sig_fs(i, _):
        pl.semaphore_signal(barrier, inc=1, device_id=((fs + i) % 32, tp), device_id_type=MESH)
        return 0

    def sig_tp(i, _):
        pl.semaphore_signal(barrier, inc=1, device_id=(fs, (tp + i) % 8), device_id_type=MESH)
        return 0

    lax.fori_loop(1, 32, sig_fs, 0)
    lax.fori_loop(1, 8, sig_tp, 0)

    rows = tok_ref[pl.ds(pl.multiple_of(tp * 32, 32), 32), :].astype(f32)
    scale = lax.rsqrt(jnp.mean(rows * rows, axis=-1, keepdims=True) + 1e-6)
    yrow = pl.multiple_of(y * 32, 32)
    tk[z, pl.ds(yrow, 32), 0:2048] = (rows * scale).astype(bf16)
    tk[z, pl.ds(yrow, 32), 2048:2176] = dense_ref[pl.ds(pl.multiple_of(tp * 32, 32), 32), :]
    gain = gain_ref[...]
    yr64 = pl.multiple_of(y * 64, 64)
    sh[0, z, pl.ds(yr64, 64), :] = (sg_ref[...] * gain).astype(bf16)
    sh[1, z, pl.ds(yr64, 64), :] = (su_ref[...] * gain).astype(bf16)
    sh[2, z, pl.ds(yr64, 64), :] = sd_ref[...].astype(bf16)

    col = pl.multiple_of(tp * 128, 128)
    frow = pl.multiple_of(fs * 64, 64)

    def convert(m):
        def one(e, _):
            if m == 2:
                wsend[2, e] = ed_ref[e].astype(bf16)
            else:
                wsend[m, e] = ((eg_ref, eu_ref)[m][e] * gain).astype(bf16)
            return 0

        lax.fori_loop(0, 32, one, 0)
        w[m, pl.ds(frow, 64), pl.ds(col, 128)] = wsend[m, fs]

    convert(0)
    pl.semaphore_wait(barrier, 38)

    def a2a(m, lo, hi):
        def one(i, _):
            dz, dy = i // NY, i % NY
            peer = ((z + dz) % NZ) * NY + (y + dy) % NY
            rc(wsend.at[m, peer], w.at[m, pl.ds(frow, 64), pl.ds(col, 128)],
               send.at[A2A + m], recv.at[A2A + m], (peer, tp)).start()
            return 0

        lax.fori_loop(lo, hi, one, 0)

    def a2a_desc(m):
        return rc(wsend.at[m, pl.ds(0, 31)], wsend.at[m, pl.ds(0, 31)],
                  send.at[A2A + m], recv.at[A2A + m], (fs, tp))

    started = []

    def go(d):
        d.start()
        started.append(d)

    def tkz(zi, half=None):
        if half is None:
            return tk.at[zi, pl.ds(yrow, 32), :]
        return tk.at[zi, pl.ds(pl.multiple_of(yrow + 16 * half, 16), 16), :]

    def shz(zi, half=None):
        if half is None:
            return sh.at[:, zi]
        return sh.at[:, zi, pl.ds(128 * half, 128), :]

    def zring(k, view, base):
        br, bl = (z - k + 1 + NZ) % NZ, (z + k - 1) % NZ
        hr, hl = (None, None) if k < 4 else (0, 1)
        go(rc(view(br, hr), view(br, hr), send.at[base + k - 1], recv.at[base + k - 1], (at_z(1), tp)))
        go(rc(view(bl, hl), view(bl, hl), send.at[base + 3 + k], recv.at[base + 3 + k], (at_z(-1), tp)))

    def zwait(k, view, base):
        br, bl = (z - k + NZ) % NZ, (z + k) % NZ
        hr, hl = (None, None) if k < 4 else (0, 1)
        rc(view(br, hr), view(br, hr), send.at[base + k - 1], recv.at[base + k - 1], (fs, tp)).wait_recv()
        rc(view(bl, hl), view(bl, hl), send.at[base + 3 + k], recv.at[base + 3 + k], (fs, tp)).wait_recv()

    def tky(yi, lo=0, n=8):
        return tk.at[pl.ds(lo, n), pl.ds(pl.multiple_of(((yi + NY) % NY) * 32, 32), 32), :]

    def shy(yi, lo=0, n=8):
        return sh.at[:, z, pl.ds(pl.multiple_of(((yi + NY) % NY) * 64 + lo * 8, 32), n * 8), :]

    def yring(k, view, base):
        if k == 1:
            go(rc(view(y), view(y), send.at[base], recv.at[base], (at_y(1), tp)))
            go(rc(view(y), view(y), send.at[base + 1], recv.at[base + 1], (at_y(-1), tp)))
        else:
            go(rc(view(y - 1, 0, 4), view(y - 1, 0, 4), send.at[base + 2], recv.at[base + 2], (at_y(1), tp)))
            go(rc(view(y + 1, 4, 4), view(y + 1, 4, 4), send.at[base + 3], recv.at[base + 3], (at_y(-1), tp)))

    def ywait(k, view, base):
        if k == 1:
            rc(view(y - 1), view(y - 1), send.at[base], recv.at[base], (fs, tp)).wait_recv()
            rc(view(y + 1), view(y + 1), send.at[base + 1], recv.at[base + 1], (fs, tp)).wait_recv()
        else:
            rc(view(y - 2, 0, 4), view(y - 2, 0, 4), send.at[base + 2], recv.at[base + 2], (fs, tp)).wait_recv()
            rc(view(y + 2, 4, 4), view(y + 2, 4, 4), send.at[base + 3], recv.at[base + 3], (fs, tp)).wait_recv()

    def wcol(m, xi, ci, part=None):
        cc = pl.multiple_of((((xi + NX) % NX) * 2 + ci) * 128, 128)
        if part is None:
            return w.at[m, :, pl.ds(cc, 128)]
        return w.at[m, pl.ds(part * 1024, 1024), pl.ds(cc, 128)]

    def xs(m, j):
        return XAG + m * 9 + j

    def xsend(m, j, xi, part, dev):
        v = wcol(m, xi, c, part)
        go(rc(v, v, send.at[xs(m, j)], recv.at[xs(m, j)], (fs, dev)))

    def xwait(m, j, xi, ci, part):
        v = wcol(m, xi, ci, part)
        rc(v, v, send.at[xs(m, j)], recv.at[xs(m, j)], (fs, tp)).wait_recv()

    def x1(m):
        xsend(m, 0, x, None, xr)
        xsend(m, 1, x, None, xl)
        xsend(m, 4, x, None, mate)

    def x2(m):
        xwait(m, 0, x - 1, c, None)
        xsend(m, 2, x - 1, 0, xr)
        xsend(m, 5, x - 1, None, mate)
        xwait(m, 1, x + 1, c, None)
        xsend(m, 3, x + 1, 1, xl)
        xsend(m, 6, x + 1, None, mate)

    def x3(m):
        xwait(m, 2, x - 2, c, 0)
        xsend(m, 7, x - 2, 0, mate)
        xwait(m, 3, x + 2, c, 1)
        xsend(m, 8, x + 2, 1, mate)

    def x4(m):
        xwait(m, 4, x, 1 - c, None)
        xwait(m, 5, x - 1, 1 - c, None)
        xwait(m, 6, x + 1, 1 - c, None)
        xwait(m, 7, x - 2, 1 - c, 0)
        xwait(m, 8, x + 2, 1 - c, 1)


    def gate_up(m):
        def one(i, _):
            r, n = i // 4, i % 4
            lhs = tk[pl.ds(4 * r, 4), :, 0:2048].reshape(512, 2048)
            cs = pl.ds(pl.multiple_of(n * 256, 256), 256)
            acc = jnp.dot(lhs, w[m, :, cs], preferred_element_type=f32)
            rs = pl.ds(pl.multiple_of(r * 512, 512), 512)
            if m == 0:
                gbuf[rs, cs] = acc
            else:
                g = gbuf[rs, cs]
                hbuf[rs, cs] = (g / (1.0 + jnp.exp(-g)) * acc).astype(bf16)
            return 0

        lax.fori_loop(0, 8, one, 0)

    lanes = lax.broadcasted_iota(jnp.int32, (1, 128), 1)
    mine = (lanes % 32 == fs) & (lanes < 96)

    def down(half):
        def one(i, _):
            r, n = i // 4, i % 4
            cs = pl.ds(pl.multiple_of(half * 1024 + n * 256, 256), 256)
            rs = pl.ds(pl.multiple_of(r * 512, 512), 512)
            acc = lax.dot_general(hbuf[rs, :], w[2, cs, :], (((1,), (1,)), ((), ())), preferred_element_type=f32)
            wt = tk[pl.ds(4 * r, 4), :, 2048:2176].reshape(512, 128).astype(f32)
            scale = jnp.sum(jnp.where(mine, wt, 0.0), axis=1, keepdims=True)
            ob[pl.ds(4 * r, 4), :, cs] = (acc * scale).astype(bf16).reshape(4, 128, 256)
            return 0

        lax.fori_loop(0, 8, one, 0)

    def bf_add(dst, a, n):
        def one(i, _):
            rs = pl.ds(pl.multiple_of(i * 16, 16), 16)
            dst[rs, :] = (dst[rs, :].astype(f32) + a[rs, :].astype(f32)).astype(bf16)
            return 0

        lax.fori_loop(0, n, one, 0)

    CA, CB = pl.ds(0, 1024), pl.ds(1024, 1024)

    def az(k, s):
        d = (z + s * (5 - k) + NZ) % NZ
        if k == 1:
            return ob.at[d, pl.ds(0 if s == 1 else 64, 64), CA]
        return ob.at[d, :, CA]

    def az_slot(k, s):
        j = 0 if s == 1 else 1
        if k == 1:
            return ra.at[j, 0, pl.ds(0, 64), :]
        return ra.at[j, k - 1]

    def az_copy(k, s):
        q = RAZ + (0 if s == 1 else 4) + k - 1
        return rc(az(k, s), az_slot(k, s), send.at[q], recv.at[q], (at_z(s), tp))

    def az_go(k):
        go(az_copy(k, 1))
        go(az_copy(k, -1))

    def az_in(k):
        for s in (1, -1):
            az_copy(k, s).wait_recv()
            d = (z + s * (4 - k) + NZ) % NZ
            if k == 1:
                bf_add(ob.at[d, pl.ds(0 if s == 1 else 64, 64), CA], az_slot(1, s), 4)
            elif k < 4:
                bf_add(ob.at[d, :, CA], az_slot(k, s), 8)
        if k == 4:
            def one(i, _):
                rs = pl.ds(pl.multiple_of(i * 16, 16), 16)
                sa[rs, :] = (ob[z, rs, CA].astype(f32) + ra[0, 3, rs, :].astype(f32) + ra[1, 3, rs, :].astype(f32)).astype(bf16)
                return 0

            lax.fori_loop(0, 8, one, 0)

    def yrows(d, k, s):
        lo_ = ((d + NY) % NY) * 32
        if k == 1:
            return pl.ds(pl.multiple_of(lo_ + (0 if s == 1 else 16), 16), 16)
        return pl.ds(pl.multiple_of(lo_, 32), 32)

    def ay_copy(k, s):
        q = RAY + (0 if s == 1 else 2) + k - 1
        j = 0 if s == 1 else 1
        slot = ya.at[j, 0, pl.ds(0, 16), :] if k == 1 else ya.at[j, 1]
        return rc(sa.at[yrows(y + s * (3 - k), k, s), :], slot, send.at[q], recv.at[q], (at_y(s), tp))

    def ay_go(k):
        go(ay_copy(k, 1))
        go(ay_copy(k, -1))

    def ay_in1():
        for s in (1, -1):
            ay_copy(1, s).wait_recv()
            bf_add(sa.at[yrows(y + s, 1, s), :], ya.at[0 if s == 1 else 1, 0, pl.ds(0, 16), :], 1)

    def by_copy(k, s):
        q = RBY + (0 if s == 1 else 2) + k - 1
        j = 0 if s == 1 else 1
        slot = yb.at[j, 0, :, pl.ds(0, 16), :] if k == 1 else yb.at[j, 1]
        return rc(ob.at[:, yrows(y + s * (3 - k), k, s), CB], slot, send.at[q], recv.at[q], (at_y(s), tp))

    def by_go(k):
        go(by_copy(k, 1))
        go(by_copy(k, -1))

    def by_in(k):
        for s in (1, -1):
            by_copy(k, s).wait_recv()
        if k == 1:
            for s in (1, -1):
                def one(i, _):
                    rs = yrows(y + s, 1, s)
                    ob[i, rs, CB] = (ob[i, rs, CB].astype(f32) + yb[0 if s == 1 else 1, 0, i, 0:16, :].astype(f32)).astype(bf16)
                    return 0

                lax.fori_loop(0, 8, one, 0)
        else:
            def two(i, _):
                rs = yrows(y, 2, 1)
                ob[i, rs, CB] = (ob[i, rs, CB].astype(f32) + yb[0, 1, i].astype(f32) + yb[1, 1, i].astype(f32)).astype(bf16)
                return 0

            lax.fori_loop(0, 8, two, 0)

    def bz_rows(k, s):
        if k == 1:
            return pl.ds(pl.multiple_of(yrow + (0 if s == 1 else 16), 16), 16)
        return pl.ds(yrow, 32)

    def bz_slot(k, s):
        j = 0 if s == 1 else 1
        return zb.at[j, 0, pl.ds(0, 16), :] if k == 1 else zb.at[j, k - 1]

    def bz_copy(k, s):
        q = RBZ + (0 if s == 1 else 4) + k - 1
        d = (z + s * (5 - k) + NZ) % NZ
        return rc(ob.at[d, bz_rows(k, s), CB], bz_slot(k, s), send.at[q], recv.at[q], (at_z(s), tp))

    def bz_go(k):
        go(bz_copy(k, 1))
        go(bz_copy(k, -1))

    def bz_in(k):
        for s in (1, -1):
            bz_copy(k, s).wait_recv()
            d = (z + s * (4 - k) + NZ) % NZ
            if k < 4:
                bf_add(ob.at[d, bz_rows(k, s), CB], bz_slot(k, s), 1 if k == 1 else 2)

    def shared():
        cg = sh[0].reshape(2048, 128)
        cu = sh[1].reshape(2048, 128)
        nrm = nb[...]
        g = jnp.dot(nrm, cg, preferred_element_type=f32)
        u = jnp.dot(nrm, cu, preferred_element_type=f32)
        h = (g / (1.0 + jnp.exp(-g)) * u).astype(bf16)

        def one(i, _):
            cd = sh[2, i]
            cs = pl.ds(pl.multiple_of(i * 256, 256), 256)
            sp[:, cs] = lax.dot_general(h, cd, (((1,), (1,)), ((), ())), preferred_element_type=f32).astype(bf16)
            return 0

        lax.fori_loop(0, 8, one, 0)
        trow = pl.ds(pl.multiple_of(tp * 32, 32), 32)

        def give(i, _):
            to = (tp + i) % 8
            rc(sp.at[pl.ds(pl.multiple_of(to * 32, 32), 32), :], sr.at[tp], send.at[SPX], recv.at[SPX], (fs, to)).start()
            return 0

        lax.fori_loop(1, 8, give, 0)
        sr[tp] = sp[trow, :]

    def spx_all():
        return rc(sr.at[pl.ds(0, 7)], sr.at[pl.ds(0, 7)], send.at[SPX], recv.at[SPX], (fs, tp))

    def normalize_all(i, _):
        rs = pl.ds(pl.multiple_of(i * 32, 32), 32)
        v = tok_ref[rs, :].astype(f32)
        nb[rs, :] = (v * lax.rsqrt(jnp.mean(v * v, axis=-1, keepdims=True) + 1e-6)).astype(bf16)
        return 0

    a2a(0, 1, 32)
    zring(1, tkz, TOKZ)
    convert(1)
    convert(2)
    a2a_desc(0).wait_recv()
    x1(0)
    zwait(1, tkz, TOKZ)
    zring(2, tkz, TOKZ)
    a2a(1, 1, 8)
    zwait(2, tkz, TOKZ)
    zring(3, tkz, TOKZ)
    a2a(1, 8, 16)
    zwait(3, tkz, TOKZ)
    zring(4, tkz, TOKZ)
    a2a(1, 16, 24)
    zwait(4, tkz, TOKZ)
    yring(1, tky, TOKY)
    a2a(1, 24, 32)
    yring(1, shy, SHY)
    lax.fori_loop(0, 8, normalize_all, 0)
    x2(0)
    a2a_desc(1).wait_recv()
    x1(1)
    a2a(2, 1, 32)
    ywait(1, shy, SHY)
    yring(2, shy, SHY)
    x3(0)
    a2a_desc(2).wait_recv()
    x1(2)
    ywait(2, shy, SHY)
    zring(1, shz, SHZ)
    x2(1)
    zwait(1, shz, SHZ)
    zring(2, shz, SHZ)
    ywait(1, tky, TOKY)
    yring(2, tky, TOKY)
    x3(1)
    zwait(2, shz, SHZ)
    zring(3, shz, SHZ)
    x4(0)
    zwait(3, shz, SHZ)
    zring(4, shz, SHZ)
    ywait(2, tky, TOKY)
    outs = [
        pltpu.make_async_copy(w.at[0, :, pl.ds(col, 128)], sg_out, loc.at[0]),
        pltpu.make_async_copy(w.at[1, :, pl.ds(col, 128)], su_out, loc.at[1]),
        pltpu.make_async_copy(w.at[2, :, pl.ds(col, 128)], sd_out, loc.at[2]),
    ]
    for o in outs:
        o.start()
    gate_up(0)
    x2(2)
    x4(1)
    gate_up(1)
    x3(2)
    zwait(4, shz, SHZ)
    cm = pltpu.make_async_copy(sh, cm_out, loc.at[3])
    cm.start()
    x4(2)
    down(0)
    az_go(1)
    down(1)
    by_go(1)
    shared()
    az_in(1)
    az_go(2)
    by_in(1)
    by_go(2)
    az_in(2)
    az_go(3)
    az_in(3)
    az_go(4)
    by_in(2)
    bz_go(1)
    bz_in(1)
    bz_go(2)
    az_in(4)
    ay_go(1)
    bz_in(2)
    bz_go(3)
    ay_in1()
    ay_go(2)
    bz_in(3)
    bz_go(4)
    spx_all().wait_recv()
    for s in (1, -1):
        ay_copy(2, s).wait_recv()
    bz_in(4)

    def finish(i, _):
        rs = pl.ds(pl.multiple_of(i * 16, 16), 16)
        rs_y = pl.ds(pl.multiple_of(yrow + i * 16, 16), 16)
        a = sa[rs_y, :].astype(f32) + ya[0, 1, rs, :].astype(f32) + ya[1, 1, rs, :].astype(f32)
        b = ob[z, rs_y, CB].astype(f32) + zb[0, 3, rs, :].astype(f32) + zb[1, 3, rs, :].astype(f32)
        for q in range(8):
            a = a + sr[q, rs, 0:1024].astype(f32)
            b = b + sr[q, rs, 1024:2048].astype(f32)
        for q in range(4):
            fin[q, rs, :] = a[:, q * 256 : q * 256 + 256].astype(bf16)
            fin[4 + q, rs, :] = b[:, q * 256 : q * 256 + 256].astype(bf16)
        return 0

    lax.fori_loop(0, 2, finish, 0)

    def give(i, _):
        to = (tp + i) % 8
        rc(fin.at[to], lo.at[tp], send.at[FIN], recv.at[FIN], (fs, to)).start()
        return 0

    lax.fori_loop(1, 8, give, 0)
    lo[tp] = fin[tp]
    fin_all = rc(fin.at[pl.ds(0, 7)], lo.at[pl.ds(0, 7)], send.at[FIN], recv.at[FIN], (fs, tp))
    for m in range(3):
        a2a_desc(m).wait_send()
    for d in started:
        d.wait_send()
    spx_all().wait_send()
    for o in outs:
        o.wait()
    cm.wait()
    fin_all.wait_recv()
    last = pltpu.make_async_copy(lo, lo_out, loc.at[4])
    last.start()
    fin_all.wait_send()
    last.wait()


def fused(tokens, dense3, gain, eg, eu, ed, sg, su, sd):
    any_ = pl.BlockSpec(memory_space=pl.ANY)
    vm = pl.BlockSpec(memory_space=pltpu.VMEM)
    V = pltpu.VMEM
    return pl.pallas_call(
        kernel,
        out_shape=[jax.ShapeDtypeStruct((8, 32, 256), bf16)]
        + [jax.ShapeDtypeStruct((2048, 128), bf16)] * 3
        + [jax.ShapeDtypeStruct((3, 8, 256, 128), bf16)],
        in_specs=[vm] * 9,
        out_specs=[any_] * 5,
        scratch_shapes=[
            V((3, 32, 64, 128), bf16),
            V((3, 2048, 1024), bf16),
            V((8, 128, COLS), bf16),
            V((3, 8, 256, 128), bf16),
            V((256, 2048), bf16),
            V((1024, 1024), f32),
            V((1024, 1024), bf16),
            V((8, 128, 2048), bf16),
            V((2, 4, 128, 1024), bf16),
            V((2, 2, 32, 1024), bf16),
            V((2, 2, 8, 32, 1024), bf16),
            V((2, 4, 32, 1024), bf16),
            V((128, 1024), bf16),
            V((256, 2048), bf16),
            V((8, 32, 2048), bf16),
            V((8, 32, 256), bf16),
            V((8, 32, 256), bf16),
            pltpu.SemaphoreType.DMA((NSEM,)),
            pltpu.SemaphoreType.DMA((NSEM,)),
            pltpu.SemaphoreType.DMA((5,)),
        ],
        compiler_params=pltpu.CompilerParams(collective_id=0, has_side_effects=True, vmem_limit_bytes=60 * 2**20),
    )(tokens, dense3, gain, eg, eu, ed, sg, su, sd)


def body(tokens, routes, route_weights, norm_gain, expert_gate, expert_up, expert_down, shared_gate, shared_up, shared_down):
    experts = jnp.arange(32, dtype=jnp.int32)
    hits = routes[:, :, None] == experts[None, None, :]
    dense = jnp.sum(jnp.where(hits, route_weights[:, :, None], 0.0), axis=1)
    high = lax.reduce_precision(dense, 8, 7)
    mid = lax.reduce_precision(dense - high, 8, 7)
    low = dense - high - mid
    dense3 = jnp.concatenate([high, mid, low, jnp.zeros_like(low)], axis=1).astype(bf16)
    gain = jnp.broadcast_to(norm_gain[:, None], (64, 128))
    lo, sg, su, sd, cm = fused(tokens, dense3, gain, expert_gate, expert_up, expert_down, shared_gate, shared_up, shared_down)
    cm = cm.reshape(3, 2048, 128)
    return lo.reshape(256, 256), sg[None], su[None], sd[None], cm[0], cm[1], cm[2]


def solution(mesh):
    return jax.shard_map(
        body,
        mesh=mesh,
        in_specs=(P("fs", None), P("fs", None), P("fs", None), P("fs"), P(None, "fs", "tp"), P(None, "fs", "tp"), P(None, "fs", "tp"), P("fs", "tp"), P("fs", "tp"), P("fs", "tp")),
        out_specs=(P("fs", "tp"), P("fs", None, "tp"), P("fs", None, "tp"), P("fs", None, "tp"), P(None, "tp"), P(None, "tp"), P(None, "tp")),
        check_vma=False,
    )
```

time: 529 us -> 180 us (0.34)
  waiting for transfers between devices: 396 us -> 0 us
  Pallas kernels: 0 us -> 170 us
  blocking collectives: 66.4 us -> 0 us
  matrix products: 27.6 us -> 0 us
  between operations: 14 us -> 0.7 us
  starting transfers between devices: 10 us -> 0 us
  other arithmetic: 8.9 us -> 1.53 us
    reduce_scatter x2 -> x0, waiting for transfers between devices: 233 us -> none  [the longest x1 224 us: body(): routed = lax.psum_scatter(weighted, 'fs', scatter_dimension=0, tiled=True)]
    pallas_call x0 -> x1, Pallas kernels: none -> 170 us  [fused(): pl.pallas_call(kernel, out_shape=[jax.ShapeDtypeStruct((8, 32, 256), bf16...]
    all_gather x3 -> x0, waiting for transfers between devices: 159 us -> none  [the longest x1 79.8 us: body(): rows = lax.all_gather(own_rows, 'fs', axis=0, tiled=True)]
    all_to_all x2 -> x0, blocking collectives: 66.4 us -> none  [the longest x1 52.6 us: body(): mine = lax.all_to_all(packed, 'fs', split_axis=0, concat_axis=1, tiled=True)]
    dot_general x4 -> x0, matrix products: 27.6 us -> none  [the longest x1 15.5 us: body(): jnp.einsum('rbh,bdh->rd', hidden, whole[:, :, 2 * width:], preferred_elem...]
    all_to_all x1 -> x0, starting transfers between devices: 9.84 us -> none  [body(): lax.all_to_all(final, 'tp', split_axis=1, concat_axis=0, tiled=True)]
    convert_element_type x6 -> x0, other arithmetic: 5.81 us -> none  [the longest x1 1.5 us: body(): (expert_gate * gain_rows).astype(bf16)]
  transfers between devices with their start and end apart: 6 -> 0, of which waited for: 6 -> 0; matrix products, arithmetic and copies ran while one was open for 7% -> 0% of each run, Pallas kernels for 0% -> 0%
where the time goes in v2:
time: 180 us
  Pallas kernels  170 us (94%)
  local copies, waits for them, and re-layouts  7.3 us (4%)
    pallas_call x1, Pallas kernels, fused(): pl.pallas_call(kernel, out_shape=[jax.ShapeDtypeStruct((8, 32, 256), bf16...  170 us

profile of v2, /device:TPU:1, one launch (start us, length us, event | category | flops | bytes accessed | tf_op | source)
XLA Modules:
  0.0 179.9 jit_solution(17527580111309948934)
XLA Ops:
  0.6 0.1 pad.3.clone
  0.7 0.7 select_reduce_fusion
  1.5 1.3 broadcast_in_dim.36.gain_ref
  2.8 0.1 copy.22
  2.9 0.1 copy.21
  3.1 0.7 maximum_maximum_fusion.dense_ref
  3.8 170.4 %shard_map.153 = (bf16[8,32,256]{2,1,0:T(8,128)(2,1)}, bf16[2048,128]{1,0:T(8,128)(2,1)}, bf16[2048,128]{1,0:T(8,128)(2,1)}, bf16[2048,128]{1,0:T(8,128)(2,1)}, bf16[3,8,256,128]{3,2,1,0:T(8,128)(2,1)}) custom-call(bf16[256,2048]{1,0:T(8,128)(2,1)} %tok_ref.1, bf16[256,128]{1,0:T(8,128)(2,1)} %maximum_maximum_fusion.dense_ref, ...), custom_call_target="tpu_custom_call" | custom-call | tf_op jit(solution)/shard_map/pallas_call | solution.py:520
  174.2 0.0 copy-start.3
  174.2 0.0 copy-start.2
  174.2 0.0 copy-start.1
  174.2 2.6 %fusion.1 = (bf16[1,8,256,128]{3,2,1,0:T(8,128)(2,1)}, bf16[1,8,256,128]{3,2,1,0:T(8,128)(2,1)}, bf16[1,8,256,128]{3,2,1,0:T(8,128)(2,1)}) fusion(bf16[3,8,256,128]{3,2,1,0:T(8,128)(2,1)} %get-tuple-element.16), kind=kLoop, calls=%fused_computation.6 | loop fusion | bytes 3145728 | tf_op jit(solution)/shard_map/slice | solution.py:564
  176.9 0.0 copy-start
  176.9 0.0 copy-done.3
  176.9 0.7 copy.28
  177.5 0.0 copy-done.2
  177.5 0.8 copy.29
  178.3 0.0 copy-done.1
  178.3 0.8 copy.30
  179.1 0.0 copy-done
  179.1 0.8 copy.31
  (3 shorter events, 0.0 us)
Async XLA Ops:
  174.2 2.7 %copy-start.3 = (bf16[8,32,256]{2,1,0:T(8,128)(2,1)S(1)}, bf16[8,32,256]{2,1,0:T(8,128)(2,1)}, u32[]{:S(2)}) copy-start(bf16[8,32,256]{2,1,0:T(8,128)(2,1)} %get-tuple-element.12) | copy-start | bytes 393220
  174.2 3.3 %copy-start.2 = (bf16[2048,128]{1,0:T(8,128)(2,1)S(1)}, bf16[2048,128]{1,0:T(8,128)(2,1)}, u32[]{:S(2)}) copy-start(bf16[2048,128]{1,0:T(8,128)(2,1)} %get-tuple-element.13) | copy-start | bytes 1572868
  174.2 4.1 %copy-start.1 = (bf16[2048,128]{1,0:T(8,128)(2,1)S(1)}, bf16[2048,128]{1,0:T(8,128)(2,1)}, u32[]{:S(2)}) copy-start(bf16[2048,128]{1,0:T(8,128)(2,1)} %get-tuple-element.14) | copy-start | bytes 1572868
  176.9 2.3 %copy-start = (bf16[2048,128]{1,0:T(8,128)(2,1)S(1)}, bf16[2048,128]{1,0:T(8,128)(2,1)}, u32[]{:S(2)}) copy-start(bf16[2048,128]{1,0:T(8,128)(2,1)} %get-tuple-element.15) | copy-start | bytes 1572868

commit v3 on v2

v3 whole, which is shorter than its diff:
```python
import functools
import jax
import jax.numpy as jnp
from jax import lax
from jax.experimental import pallas as pl
from jax.experimental.pallas import tpu as pltpu
from jax.sharding import PartitionSpec as P

MESH = pl.DeviceIdType.MESH
bf16, f32 = jnp.bfloat16, jnp.float32
NZ, NY, NX = 8, 4, 4
COLS = 2048 + 128

A2A = 0
TOKZ = 6
TOKY = 14
SHZ = 38
SHY = 46
XAG = 50
RAZ = 104
RAY = 120
RBY = 128
RBZ = 136
SPX = 152
FIN = 153
NSEM = 154


def rc(src, dst, ssem, rsem, dev):
    return pltpu.make_async_remote_copy(
        src_ref=src, dst_ref=dst, send_sem=ssem, recv_sem=rsem, device_id=dev, device_id_type=MESH
    )


def kernel(
    tok_hbm, rt_hbm, rw_hbm, gn_hbm, eg_hbm, eu_hbm, ed_hbm, sg_hbm, su_hbm, sd_hbm,
    lo_out, sg_out, su_out, sd_out, cg_out, cu_out, cd_out,
    tok_ref, rt_ref, rw_ref, gn_ref, ew_ref, sw_ref,
    wsend, w, tk, sh, nb, gbuf, hbuf, ob, ra, ya, yb, zb, sa, sp, sr, fin, lo, send, recv, loc,
):
    fs, tp = lax.axis_index("fs"), lax.axis_index("tp")
    z, y = fs // NY, fs % NY
    x, c = tp // 2, tp % 2

    def at_z(d):
        return ((z + d + NZ) % NZ) * NY + y

    def at_y(d):
        return z * NY + (y + d + NY) % NY

    xr, xl = ((x + 1) % NX) * 2 + c, ((x + NX - 1) % NX) * 2 + c
    mate = x * 2 + 1 - c

    barrier = pltpu.get_barrier_semaphore()

    def sig_fs(i, _):
        pl.semaphore_signal(barrier, inc=1, device_id=((fs + i) % 32, tp), device_id_type=MESH)
        return 0

    def sig_tp(i, _):
        pl.semaphore_signal(barrier, inc=1, device_id=(fs, (tp + i) % 8), device_id_type=MESH)
        return 0

    fetch = [
        pltpu.make_async_copy(a, b, loc.at[n])
        for n, (a, b) in enumerate(
            [
                (gn_hbm, gn_ref), (eg_hbm, ew_ref.at[0]), (tok_hbm, tok_ref), (rt_hbm, rt_ref), (rw_hbm, rw_ref),
                (sg_hbm, sw_ref.at[0]), (su_hbm, sw_ref.at[1]), (sd_hbm, sw_ref.at[2]),
                (eu_hbm, ew_ref.at[1]), (ed_hbm, ew_ref.at[2]),
            ]
        )
    ]
    for f in fetch:
        f.start()
    lax.fori_loop(1, 32, sig_fs, 0)
    lax.fori_loop(1, 8, sig_tp, 0)

    yrow = pl.multiple_of(y * 32, 32)
    yr64 = pl.multiple_of(y * 64, 64)
    col = pl.multiple_of(tp * 128, 128)
    srow = pl.ds(pl.multiple_of(tp * 32, 32), 32)

    fetch[0].wait()
    eye = lax.broadcasted_iota(jnp.int32, (64, 64), 0) == lax.broadcasted_iota(jnp.int32, (64, 64), 1)
    gain = jnp.sum(jnp.where(eye, gn_ref[...], 0.0), axis=1, keepdims=True)

    def convert(m):
        def one(e, _):
            if m == 2:
                wsend[2, e] = ew_ref[2, e].astype(bf16)
            else:
                wsend[m, e] = (ew_ref[m, e] * gain).astype(bf16)
            return 0

        lax.fori_loop(0, 32, one, 0)
        w[m, fs, :, pl.ds(col, 128)] = wsend[m, fs]

    fetch[1].wait()
    convert(0)

    for n in (2, 3, 4):
        fetch[n].wait()
    rows = tok_ref[srow, :].astype(f32)
    scale = lax.rsqrt(jnp.mean(rows * rows, axis=-1, keepdims=True) + 1e-6)
    tk[z, pl.ds(yrow, 32), 0:2048] = (rows * scale).astype(bf16)
    lanes = lax.broadcasted_iota(jnp.int32, (1, 128), 1)
    expert = lax.broadcasted_iota(jnp.int32, (128, 1), 0)
    dense = jnp.zeros((128, 256), f32)
    for k in range(6):
        dense = dense + jnp.where(rt_ref[k : k + 1, :] == expert % 32, rw_ref[k : k + 1, :], 0.0)
    high = dense.astype(bf16).astype(f32)
    mid = (dense - high).astype(bf16).astype(f32)
    low = dense - high - mid
    terms = jnp.where(expert < 32, high, jnp.where(expert < 64, mid, jnp.where(expert < 96, low, 0.0)))
    pick = lax.broadcasted_iota(jnp.int32, (32, 256), 1) == lax.broadcasted_iota(jnp.int32, (32, 256), 0) + tp * 32
    tk[z, pl.ds(yrow, 32), 2048:2176] = lax.dot_general(
        jnp.where(pick, 1.0, 0.0).astype(bf16), terms.astype(bf16), (((1,), (1,)), ((), ())), preferred_element_type=f32
    ).astype(bf16)
    for n in (5, 6, 7):
        fetch[n].wait()
    sh[0, z, pl.ds(yr64, 64), :] = (sw_ref[0] * gain).astype(bf16)
    sh[1, z, pl.ds(yr64, 64), :] = (sw_ref[1] * gain).astype(bf16)
    sh[2, z, pl.ds(yr64, 64), :] = sw_ref[2].astype(bf16)
    pl.semaphore_wait(barrier, 38)

    def a2a(j):
        m, h = j // 2, pl.ds(32 * (j % 2), 32)

        def one(i, _):
            dz, dy = i // NY, i % NY
            peer = ((z + dz) % NZ) * NY + (y + dy) % NY
            rc(wsend.at[m, peer, h], w.at[m, fs, h, pl.ds(col, 128)],
               send.at[A2A + j], recv.at[A2A + j], (peer, tp)).start()
            return 0

        lax.fori_loop(1, 32, one, 0)

    def a2a_desc(j):
        v = wsend.at[j // 2, pl.ds(0, 31), pl.ds(32 * (j % 2), 32)]
        return rc(v, v, send.at[A2A + j], recv.at[A2A + j], (fs, tp))

    started = []

    def go(d):
        d.start()
        started.append(d)

    def tkz(zi, half=None):
        if half is None:
            return tk.at[zi, pl.ds(yrow, 32), :]
        return tk.at[zi, pl.ds(pl.multiple_of(yrow + 16 * half, 16), 16), :]

    def shz(zi, half=None):
        if half is None:
            return sh.at[:, zi]
        return sh.at[:, zi, pl.ds(128 * half, 128), :]

    def zring(k, view, base):
        br, bl = (z - k + 1 + NZ) % NZ, (z + k - 1) % NZ
        hr, hl = (None, None) if k < 4 else (0, 1)
        go(rc(view(br, hr), view(br, hr), send.at[base + k - 1], recv.at[base + k - 1], (at_z(1), tp)))
        go(rc(view(bl, hl), view(bl, hl), send.at[base + 3 + k], recv.at[base + 3 + k], (at_z(-1), tp)))

    def zwait(k, view, base):
        br, bl = (z - k + NZ) % NZ, (z + k) % NZ
        hr, hl = (None, None) if k < 4 else (0, 1)
        rc(view(br, hr), view(br, hr), send.at[base + k - 1], recv.at[base + k - 1], (fs, tp)).wait_recv()
        rc(view(bl, hl), view(bl, hl), send.at[base + 3 + k], recv.at[base + 3 + k], (fs, tp)).wait_recv()

    def tkb(o, yi):
        return tk.at[(z + o) % NZ, pl.ds(pl.multiple_of(((yi + NY) % NY) * 32, 32), 32), :]

    def ty1(*offsets):
        for o in offsets:
            go(rc(tkb(o, y), tkb(o, y), send.at[TOKY + o], recv.at[TOKY + o], (at_y(1), tp)))
            go(rc(tkb(o, y), tkb(o, y), send.at[TOKY + 8 + o], recv.at[TOKY + 8 + o], (at_y(-1), tp)))

    def ty_wait(n, o, yi):
        rc(tkb(o, yi), tkb(o, yi), send.at[n], recv.at[n], (fs, tp)).wait_recv()

    def ty2(*offsets):
        for o in offsets:
            s = 1 if o < 4 else -1
            ty_wait(TOKY + (0 if o < 4 else 8) + o, o, y - s)
            go(rc(tkb(o, y - s), tkb(o, y - s), send.at[TOKY + 16 + o], recv.at[TOKY + 16 + o], (at_y(s), tp)))

    def ty_in1():
        for o in range(8):
            s = 1 if o < 4 else -1
            ty_wait(TOKY + (8 if o < 4 else 0) + o, o, y + s)

    def ty_in2():
        for o in range(8):
            ty_wait(TOKY + 16 + o, o, y + 2)

    def shy(yi, lo=0, n=8):
        return sh.at[:, z, pl.ds(pl.multiple_of(((yi + NY) % NY) * 64 + lo * 8, 32), n * 8), :]

    def yring(k, view, base):
        if k == 1:
            go(rc(view(y), view(y), send.at[base], recv.at[base], (at_y(1), tp)))
            go(rc(view(y), view(y), send.at[base + 1], recv.at[base + 1], (at_y(-1), tp)))
        else:
            go(rc(view(y - 1, 0, 4), view(y - 1, 0, 4), send.at[base + 2], recv.at[base + 2], (at_y(1), tp)))
            go(rc(view(y + 1, 4, 4), view(y + 1, 4, 4), send.at[base + 3], recv.at[base + 3], (at_y(-1), tp)))

    def ywait(k, view, base):
        if k == 1:
            rc(view(y - 1), view(y - 1), send.at[base], recv.at[base], (fs, tp)).wait_recv()
            rc(view(y + 1), view(y + 1), send.at[base + 1], recv.at[base + 1], (fs, tp)).wait_recv()
        else:
            rc(view(y - 2, 0, 4), view(y - 2, 0, 4), send.at[base + 2], recv.at[base + 2], (fs, tp)).wait_recv()
            rc(view(y + 2, 4, 4), view(y + 2, 4, 4), send.at[base + 3], recv.at[base + 3], (fs, tp)).wait_recv()

    def wcol(j, xi, ci, part=None):
        cc = pl.multiple_of((((xi + NX) % NX) * 2 + ci) * 128, 128)
        m, h = j // 2, pl.ds(32 * (j % 2), 32)
        if part is None:
            return w.at[m, :, h, pl.ds(cc, 128)]
        return w.at[m, pl.ds(part * 16, 16), h, pl.ds(cc, 128)]

    def xs(m, j):
        return XAG + m * 9 + j

    def xsend(m, j, xi, part, dev):
        v = wcol(m, xi, c, part)
        go(rc(v, v, send.at[xs(m, j)], recv.at[xs(m, j)], (fs, dev)))

    def xwait(m, j, xi, ci, part):
        v = wcol(m, xi, ci, part)
        rc(v, v, send.at[xs(m, j)], recv.at[xs(m, j)], (fs, tp)).wait_recv()

    def x1(m):
        xsend(m, 0, x, None, xr)
        xsend(m, 1, x, None, xl)
        xsend(m, 4, x, None, mate)

    def x2(m):
        xwait(m, 0, x - 1, c, None)
        xsend(m, 2, x - 1, 0, xr)
        xsend(m, 5, x - 1, None, mate)
        xwait(m, 1, x + 1, c, None)
        xsend(m, 3, x + 1, 1, xl)
        xsend(m, 6, x + 1, None, mate)

    def x3(m):
        xwait(m, 2, x - 2, c, 0)
        xsend(m, 7, x - 2, 0, mate)
        xwait(m, 3, x + 2, c, 1)
        xsend(m, 8, x + 2, 1, mate)

    def x4(m):
        xwait(m, 4, x, 1 - c, None)
        xwait(m, 5, x - 1, 1 - c, None)
        xwait(m, 6, x + 1, 1 - c, None)
        xwait(m, 7, x - 2, 1 - c, 0)
        xwait(m, 8, x + 2, 1 - c, 1)


    def gate_up(m, dy):
        rs = pl.ds(pl.multiple_of(((y + dy + NY) % NY) * 32, 32), 32)

        def one(n, _):
            lhs = tk[:, rs, 0:2048].reshape(256, 2048)
            cs = pl.ds(pl.multiple_of(n * 512, 512), 512)
            acc = jnp.dot(lhs, w[m, :, :, cs].reshape(2048, 512), preferred_element_type=f32)
            acc = acc.reshape(8, 32, 512)
            if m == 0:
                gbuf[:, rs, cs] = acc
            else:
                g = gbuf[:, rs, cs]
                hbuf[:, rs, cs] = (g / (1.0 + jnp.exp(-g)) * acc).astype(bf16)
            return 0

        lax.fori_loop(0, 2, one, 0)

    mine = (lanes % 32 == fs) & (lanes < 96)

    def down(quarter):
        def one(r, _):
            cs = pl.ds(quarter * 512, 512)
            wd = w[2, pl.ds(quarter * 8, 8)].reshape(512, 1024)
            h = hbuf[pl.ds(4 * r, 4)].reshape(512, 1024)
            acc = lax.dot_general(h, wd, (((1,), (1,)), ((), ())), preferred_element_type=f32)
            wt = tk[pl.ds(4 * r, 4), :, 2048:2176].reshape(512, 128).astype(f32)
            scale = jnp.sum(jnp.where(mine, wt, 0.0), axis=1, keepdims=True)
            ob[pl.ds(4 * r, 4), :, cs] = (acc * scale).astype(bf16).reshape(4, 128, 512)
            return 0

        lax.fori_loop(0, 2, one, 0)

    def bf_add(dst, a, n):
        def one(i, _):
            rs = pl.ds(pl.multiple_of(i * 16, 16), 16)
            dst[rs, :] = (dst[rs, :].astype(f32) + a[rs, :].astype(f32)).astype(bf16)
            return 0

        lax.fori_loop(0, n, one, 0)

    def ca(q):
        return pl.ds(q * 512, 512)

    def cb(q):
        return pl.ds(1024 + q * 512, 512)

    def az(q, k, s):
        d = (z + s * (5 - k) + NZ) % NZ
        if k == 1:
            return ob.at[d, pl.ds(0 if s == 1 else 64, 64), ca(q)]
        return ob.at[d, :, ca(q)]

    def az_slot(q, k, s):
        j = 0 if s == 1 else 1
        if k == 1:
            return ra.at[j, 0, pl.ds(0, 64), ca(q)]
        return ra.at[j, k - 1, :, ca(q)]

    def az_copy(q, k, s):
        n = RAZ + 8 * q + (0 if s == 1 else 4) + k - 1
        return rc(az(q, k, s), az_slot(q, k, s), send.at[n], recv.at[n], (at_z(s), tp))

    def az_go(q, k):
        go(az_copy(q, k, 1))
        go(az_copy(q, k, -1))

    def az_in(q, k):
        for s in (1, -1):
            az_copy(q, k, s).wait_recv()
            d = (z + s * (4 - k) + NZ) % NZ
            if k == 1:
                bf_add(ob.at[d, pl.ds(0 if s == 1 else 64, 64), ca(q)], az_slot(q, 1, s), 4)
            elif k < 4:
                bf_add(ob.at[d, :, ca(q)], az_slot(q, k, s), 8)
        if k == 4:
            def one(i, _):
                rs = pl.ds(pl.multiple_of(i * 16, 16), 16)
                c_ = ca(q)
                sa[rs, c_] = (ob[z, rs, c_].astype(f32) + ra[0, 3, rs, c_].astype(f32) + ra[1, 3, rs, c_].astype(f32)).astype(bf16)
                return 0

            lax.fori_loop(0, 8, one, 0)

    def yrows(d, k, s):
        lo_ = ((d + NY) % NY) * 32
        if k == 1:
            return pl.ds(pl.multiple_of(lo_ + (0 if s == 1 else 16), 16), 16)
        return pl.ds(pl.multiple_of(lo_, 32), 32)

    def ay_copy(q, d):
        n = RAY + 4 * q + d
        src = sa.at[pl.ds(pl.multiple_of(((y + d) % NY) * 32, 32), 32), ca(q)]
        return rc(src, ya.at[d - 1, :, ca(q)], send.at[n], recv.at[n], (at_y(d), tp))

    def ay_go(q):
        for d in (2, 1, 3):
            go(ay_copy(q, d))

    def ay_in(q):
        for d in (1, 2, 3):
            ay_copy(q, d).wait_recv()

    def by_slot(q, k, s):
        j = 0 if s == 1 else 1
        return yb.at[j, 0, :, pl.ds(0, 16), ca(q)] if k == 1 else yb.at[j, 1, :, :, ca(q)]

    def by_copy(q, k, s):
        n = RBY + 4 * q + (0 if s == 1 else 2) + k - 1
        return rc(ob.at[:, yrows(y + s * (3 - k), k, s), cb(q)], by_slot(q, k, s), send.at[n], recv.at[n], (at_y(s), tp))

    def by_go(q, k):
        go(by_copy(q, k, 1))
        go(by_copy(q, k, -1))

    def by_in(q, k):
        for s in (1, -1):
            by_copy(q, k, s).wait_recv()
            if k == 1:
                rs, j = yrows(y + s, 1, s), 0 if s == 1 else 1

                def one(i, _):
                    ob[i, rs, cb(q)] = (ob[i, rs, cb(q)].astype(f32) + yb[j, 0, i, 0:16, ca(q)].astype(f32)).astype(bf16)
                    return 0

                lax.fori_loop(0, 8, one, 0)
        if k == 2:
            rs2 = yrows(y, 2, 1)

            def two(i, _):
                ob[i, rs2, cb(q)] = (ob[i, rs2, cb(q)].astype(f32) + yb[0, 1, i, :, ca(q)].astype(f32) + yb[1, 1, i, :, ca(q)].astype(f32)).astype(bf16)
                return 0

            lax.fori_loop(0, 8, two, 0)

    def bz_copy(q, part, s):
        j = 0 if s == 1 else 1
        n = RBZ + 8 * q + 4 * j + part
        d = (z + s * (4 - part) + NZ) % NZ
        rows = pl.ds(yrow, 32)
        slot = zb.at[j, part, :, ca(q)]
        if part == 0:
            rows = pl.ds(pl.multiple_of(yrow + 16 * j, 16), 16)
            slot = zb.at[j, 0, pl.ds(0, 16), ca(q)]
        to = at_z(s) if part == 3 else at_z(2 * s)
        return rc(ob.at[d, rows, cb(q)], slot, send.at[n], recv.at[n], (to, tp))

    def bz_go(q, *parts):
        for part in parts:
            go(bz_copy(q, part, 1))
            go(bz_copy(q, part, -1))

    def bz_in1(q):
        for s in (1, -1):
            j = 0 if s == 1 else 1
            bz_copy(q, 1, s).wait_recv()
            bf_add(ob.at[(z + s + NZ) % NZ, pl.ds(yrow, 32), cb(q)], zb.at[j, 1, :, ca(q)], 2)
        bz_go(q, 3)
        for s in (1, -1):
            j = 0 if s == 1 else 1
            bz_copy(q, 0, s).wait_recv()
            half = pl.ds(pl.multiple_of(yrow + 16 * j, 16), 16)
            bf_add(ob.at[(z + 2 * s + NZ) % NZ, half, cb(q)], zb.at[j, 0, pl.ds(0, 16), ca(q)], 1)
        bz_go(q, 2)

    def bz_in2(q):
        for part in (2, 3):
            for s in (1, -1):
                bz_copy(q, part, s).wait_recv()

    def shared():
        cg = sh[0].reshape(2048, 128)
        cu = sh[1].reshape(2048, 128)
        nrm = nb[...]
        g = jnp.dot(nrm, cg, preferred_element_type=f32)
        u = jnp.dot(nrm, cu, preferred_element_type=f32)
        h = (g / (1.0 + jnp.exp(-g)) * u).astype(bf16)

        def one(i, _):
            cd = sh[2, i]
            cs = pl.ds(pl.multiple_of(i * 256, 256), 256)
            sp[:, cs] = lax.dot_general(h, cd, (((1,), (1,)), ((), ())), preferred_element_type=f32).astype(bf16)
            return 0

        lax.fori_loop(0, 8, one, 0)
        trow = pl.ds(pl.multiple_of(tp * 32, 32), 32)

        def give(i, _):
            to = (tp + i) % 8
            rc(sp.at[pl.ds(pl.multiple_of(to * 32, 32), 32), :], sr.at[tp], send.at[SPX], recv.at[SPX], (fs, to)).start()
            return 0

        lax.fori_loop(1, 8, give, 0)
        sr[tp] = sp[trow, :]

    def spx_all():
        return rc(sr.at[pl.ds(0, 7)], sr.at[pl.ds(0, 7)], send.at[SPX], recv.at[SPX], (fs, tp))

    def normalize_all(i, _):
        rs = pl.ds(pl.multiple_of(i * 32, 32), 32)
        v = tok_ref[rs, :].astype(f32)
        nb[rs, :] = (v * lax.rsqrt(jnp.mean(v * v, axis=-1, keepdims=True) + 1e-6)).astype(bf16)
        return 0

    a2a(0)
    zring(1, tkz, TOKZ)
    ty1(0)
    yring(1, shy, SHY)
    fetch[8].wait()
    convert(1)
    fetch[9].wait()
    convert(2)
    a2a(1)
    zwait(1, tkz, TOKZ)
    zring(2, tkz, TOKZ)
    a2a(2)
    ty1(1, 7)
    a2a_desc(0).wait_recv()
    x1(0)
    a2a_desc(1).wait_recv()
    x1(1)
    zwait(2, tkz, TOKZ)
    zring(3, tkz, TOKZ)
    a2a(3)
    ty1(2, 6)
    x2(0)
    a2a_desc(2).wait_recv()
    x1(2)
    x2(1)
    zwait(3, tkz, TOKZ)
    zring(4, tkz, TOKZ)
    a2a(4)
    ty1(3, 5)
    x3(0)
    a2a_desc(3).wait_recv()
    x1(3)
    zwait(4, tkz, TOKZ)
    a2a(5)
    ty1(4)
    ty2(0)
    ywait(1, shy, SHY)
    yring(2, shy, SHY)
    x2(2)
    x3(1)
    ty2(1, 7)
    lax.fori_loop(0, 8, normalize_all, 0)
    a2a_desc(4).wait_recv()
    x1(4)
    ty2(2, 6)
    x2(3)
    x3(2)
    ty2(3, 5)
    ywait(2, shy, SHY)
    a2a_desc(5).wait_recv()
    x1(5)
    ty2(4)
    zring(1, shz, SHZ)
    ty_in1()
    x4(0)
    x4(1)
    gate_up(0, 0)
    x2(4)
    gate_up(0, 1)
    x3(3)
    gate_up(0, -1)
    zwait(1, shz, SHZ)
    zring(2, shz, SHZ)
    x2(5)
    x4(2)
    x4(3)
    gate_up(1, 0)
    x3(4)
    gate_up(1, 1)
    gate_up(1, -1)
    x3(5)
    zwait(2, shz, SHZ)
    zring(3, shz, SHZ)
    ty_in2()
    gate_up(0, 2)
    gate_up(1, 2)
    outs = [
        pltpu.make_async_copy(w.at[m, :, :, pl.ds(col, 128)], (sg_out, su_out, sd_out)[m], loc.at[m]) for m in range(3)
    ]
    commons = [pltpu.make_async_copy(sh.at[m], (cg_out, cu_out, cd_out)[m], loc.at[3 + m]) for m in range(3)]
    for o in outs:
        o.start()
    zwait(3, shz, SHZ)
    zring(4, shz, SHZ)
    x4(4)
    x4(5)
    down(2)
    by_go(0, 1)
    down(0)
    az_go(0, 1)
    down(3)
    by_go(1, 1)
    down(1)
    az_go(1, 1)
    by_in(0, 1)
    by_go(0, 2)
    az_in(0, 1)
    az_go(0, 2)
    by_in(1, 1)
    by_go(1, 2)
    az_in(1, 1)
    az_go(1, 2)
    zwait(4, shz, SHZ)
    shared()
    az_in(0, 2)
    az_go(0, 3)
    az_in(1, 2)
    az_go(1, 3)
    by_in(0, 2)
    bz_go(0, 1, 0)
    az_in(0, 3)
    az_go(0, 4)
    az_in(1, 3)
    az_go(1, 4)
    by_in(1, 2)
    bz_go(1, 1, 0)
    bz_in1(0)
    az_in(0, 4)
    ay_go(0)
    bz_in1(1)
    az_in(1, 4)
    ay_go(1)
    for m in range(3):
        commons[m].start()
    spx_all().wait_recv()
    ay_in(0)
    bz_in2(0)
    bz_in2(1)
    ay_in(1)

    def finish(i, _):
        rs = pl.ds(pl.multiple_of(i * 16, 16), 16)
        rs_y = pl.ds(pl.multiple_of(yrow + i * 16, 16), 16)
        a = sa[rs_y, :].astype(f32) + ya[0, rs, :].astype(f32) + ya[1, rs, :].astype(f32) + ya[2, rs, :].astype(f32)
        b = ob[z, rs_y, 1024:2048].astype(f32)
        for j in range(2):
            b = b + zb[j, 2, rs, :].astype(f32) + zb[j, 3, rs, :].astype(f32)
        for q in range(8):
            a = a + sr[q, rs, 0:1024].astype(f32)
            b = b + sr[q, rs, 1024:2048].astype(f32)
        for q in range(4):
            fin[q, rs, :] = a[:, q * 256 : q * 256 + 256].astype(bf16)
            fin[4 + q, rs, :] = b[:, q * 256 : q * 256 + 256].astype(bf16)
        return 0

    lax.fori_loop(0, 2, finish, 0)

    def give(i, _):
        to = (tp + i) % 8
        rc(fin.at[to], lo.at[tp], send.at[FIN], recv.at[FIN], (fs, to)).start()
        return 0

    lax.fori_loop(1, 8, give, 0)
    lo[tp] = fin[tp]
    fin_all = rc(fin.at[pl.ds(0, 7)], lo.at[pl.ds(0, 7)], send.at[FIN], recv.at[FIN], (fs, tp))
    for j in range(6):
        a2a_desc(j).wait_send()
    for d in started:
        d.wait_send()
    spx_all().wait_send()
    for o in outs:
        o.wait()
    for o in commons:
        o.wait()
    fin_all.wait_recv()
    last = pltpu.make_async_copy(lo, lo_out, loc.at[6])
    last.start()
    fin_all.wait_send()
    last.wait()


def fused(*args):
    any_ = pl.BlockSpec(memory_space=pl.ANY)
    V = pltpu.VMEM
    shape = jax.ShapeDtypeStruct
    return pl.pallas_call(
        kernel,
        out_shape=[shape((8, 32, 256), bf16)] + [shape((32, 64, 128), bf16)] * 3 + [shape((8, 256, 128), bf16)] * 3,
        in_specs=[any_] * 10,
        out_specs=[any_] * 7,
        scratch_shapes=[
            V((256, 2048), bf16),
            V((6, 256), jnp.int32),
            V((6, 256), f32),
            V((1, 64), f32),
            V((3, 32, 64, 128), f32),
            V((3, 64, 128), f32),
            V((3, 32, 64, 128), bf16),
            V((3, 32, 64, 1024), bf16),
            V((8, 128, COLS), bf16),
            V((3, 8, 256, 128), bf16),
            V((256, 2048), bf16),
            V((8, 128, 1024), f32),
            V((8, 128, 1024), bf16),
            V((8, 128, 2048), bf16),
            V((2, 4, 128, 1024), bf16),
            V((3, 32, 1024), bf16),
            V((2, 2, 8, 32, 1024), bf16),
            V((2, 4, 32, 1024), bf16),
            V((128, 1024), bf16),
            V((256, 2048), bf16),
            V((8, 32, 2048), bf16),
            V((8, 32, 256), bf16),
            V((8, 32, 256), bf16),
            pltpu.SemaphoreType.DMA((NSEM,)),
            pltpu.SemaphoreType.DMA((NSEM,)),
            pltpu.SemaphoreType.DMA((10,)),
        ],
        compiler_params=pltpu.CompilerParams(collective_id=0, has_side_effects=True, vmem_limit_bytes=60 * 2**20),
    )(*args)


def settle_kernel(*refs):
    n = (len(refs) - 2) // 3
    ins, outs, held = refs[:n], refs[n : 2 * n], refs[2 * n : 3 * n]
    sem_in, sem_out = refs[-2:]
    get = [pltpu.make_async_copy(ins[k], held[k], sem_in.at[k]) for k in range(n)]
    put = [pltpu.make_async_copy(held[k], outs[k], sem_out.at[k]) for k in range(n)]
    for g in get:
        g.start()
    for k in range(n):
        get[k].wait()
        put[k].start()
    for p in put:
        p.wait()


def settle(*arrays):
    any_ = pl.BlockSpec(memory_space=pl.ANY)
    n = len(arrays)
    return pl.pallas_call(
        settle_kernel,
        out_shape=[jax.ShapeDtypeStruct(a.shape, a.dtype) for a in arrays],
        in_specs=[any_] * n,
        out_specs=[any_] * n,
        scratch_shapes=[pltpu.VMEM(a.shape, a.dtype) for a in arrays]
        + [pltpu.SemaphoreType.DMA((n,)), pltpu.SemaphoreType.DMA((n,))],
        compiler_params=pltpu.CompilerParams(vmem_limit_bytes=60 * 2**20),
    )(*arrays)


def body(tokens, routes, route_weights, norm_gain, *weights):
    lo, sg, su, sd, cg, cu, cd = settle(*fused(tokens, routes.T, route_weights.T, norm_gain.reshape(1, 64), *weights))
    sample = [a.reshape(1, 2048, 128) for a in (sg, su, sd)]
    common = [a.reshape(2048, 128) for a in (cg, cu, cd)]
    return (lo.reshape(256, 256), *sample, *common)


def solution(mesh):
    return jax.shard_map(
        body,
        mesh=mesh,
        in_specs=(P("fs", None), P("fs", None), P("fs", None), P("fs"), P(None, "fs", "tp"), P(None, "fs", "tp"), P(None, "fs", "tp"), P("fs", "tp"), P("fs", "tp"), P("fs", "tp")),
        out_specs=(P("fs", "tp"), P("fs", None, "tp"), P("fs", None, "tp"), P("fs", None, "tp"), P(None, "tp"), P(None, "tp"), P(None, "tp")),
        check_vma=False,
    )
```

time: 180 us -> 130 us (0.72)
  Pallas kernels: 170 us -> 129 us
  local copies, waits for them, and re-layouts: 7.3 us -> 0 us
    pallas_call x1 -> x2, Pallas kernels: 170 us -> 129 us  [the longest x1 126 us: fused(): pl.pallas_call(kernel, out_shape=[shape((8, 32, 256), bf16)] + [shape((32...]
    unnamed x12 -> x0, local copies, waits for them, and re-layouts: 3.05 us -> none
    slice x1 -> x0, local copies, waits for them, and re-layouts: 2.63 us -> none  [body(): cm[2]]
where the time goes in v3:
time: 130 us
  Pallas kernels  129 us (99%)
    pallas_call x1, Pallas kernels, fused(): pl.pallas_call(kernel, out_shape=[shape((8, 32, 256), bf16)] + [shape((32...  126 us
    pallas_call x1, Pallas kernels, settle(): pl.pallas_call(settle_kernel, out_shape=[jax.ShapeDtypeStruct(a.shape, a....  2.89 us

profile of v3, /device:TPU:1, one launch (start us, length us, event | category | flops | bytes accessed | tf_op | source)
XLA Modules:
  0.0 129.6 jit_solution(12881551093781368402)
XLA Ops:
  0.6 126.0 %shard_map.153 = (bf16[8,32,256]{2,1,0:T(8,128)(2,1)}, bf16[32,64,128]{2,1,0:T(8,128)(2,1)}, bf16[32,64,128]{2,1,0:T(8,128)(2,1)}, bf16[32,64,128]{2,1,0:T(8,128...) custom-call(bf16[256,2048]{1,0:T(8,128)(2,1)} %tok_hbm.1, ...), custom_call_target="tpu_custom_call" | custom-call | tf_op jit(solution)/shard_map/pallas_call | solution.py:639
  126.7 2.9 %shard_map.154 = (bf16[8,32,256]{2,1,0:T(8,128)(2,1)}, bf16[32,64,128]{2,1,0:T(8,128)(2,1)}, bf16[32,64,128]{2,1,0:T(8,128)(2,1)}, bf16[32,64,128]{2,1,0:T(8,128...) custom-call(bf16[8,32,256]{2,1,0:T(8,128)(2,1)} %get-tuple-element.21.refs_0_, ...), custom_call_target="tpu_custom_call" | custom-call | tf_op jit(solution)/shard_map/pallas_call | solution.py:694
